TPU v7x, 256 devices: a whole 4x4x8 slice. The times are simulated.
256 devices in a mesh: sp: 32 (over z, x), tp: 8 (over y, core).
Axes of the slice: x: 4, y: 4, z: 8, core: 2. Of those that a mesh axis runs over, the one named last changes fastest.
Arguments:
- resid: bfloat16 [8192, 2048], P('sp'), may hold values from -6 to 6
- query_one: bfloat16 [8192, 1024], P('sp', 'tp'), may hold values from -400 to 400
- query_two: bfloat16 [8192, 1024], P('sp', 'tp'), may hold values from -400 to 400
- key_one: bfloat16 [8192, 1024], P('sp', 'tp'), may hold values from -8 to 8
- key_two: bfloat16 [8192, 1024], P('sp', 'tp'), may hold values from -8 to 8
- values: bfloat16 [8192, 2048], P('sp', 'tp'), may hold values from -6 to 6
- documents: int32 [8192], P('sp'), may hold values from 0 to 7, never falling along the last dimension, each value on 1 to 4352 neighbouring positions
- mix_lambda: float32 [16], P('tp'), may hold values from 0.3 to 0.8
- head_gain: float32 [128], replicated, may hold values from 0.1 to 1.9
- out_weight: bfloat16 [2048, 2048], P('tp'), may hold values from -0.125 to 0.125
- ffn_gain: float32 [2048], replicated, may hold values from 0.1 to 1.9
- routes: int32 [8192, 4], P('sp'), may hold values from 0 to 255, all different within a row; in each aligned block of 256 rows (0 to 255, 256 to 511, ...) at most 8 rows name the same one
- route_weight: float32 [8192, 4], P('sp'), may hold values from 0.2 to 0.9
- expert_gate: bfloat16 [256, 2048, 512], P(('sp', 'tp')), may hold values from -0.125 to 0.125
- expert_up: bfloat16 [256, 2048, 512], P(('sp', 'tp')), may hold values from -0.125 to 0.125
- expert_down: bfloat16 [256, 512, 2048], P(('sp', 'tp')), may hold values from -0.25 to 0.25
- shared_gate: bfloat16 [2048, 512], P(None, 'tp'), may hold values from -0.125 to 0.125
- shared_up: bfloat16 [2048, 512], P(None, 'tp'), may hold values from -0.125 to 0.125
- shared_down: bfloat16 [512, 2048], P('tp'), may hold values from -0.25 to 0.25
Outputs:
- layer_out: bfloat16 [8192, 2048], P(('sp', 'tp'))
Inputs may be any that keep to these rules, and one draw needn't show every extreme that they name: `documents`: document numbers never fall along the positions; each document has 1 to 4352 positions and one has exactly 4352. `routes`: A row names 4 different experts. In each aligned block of 256 rows no expert is named by more than 8 rows, a bound that some block reaches.
All inputs are finite; a program needn't handle non-finite values.
Results may differ from a plain program's by a relative error of at most 0.018.
Values may be sent and summed in bfloat16 or wider, within the bound.
No kernel may reach another device: no remote copies, remote signals or barrier semaphores. Data moves between devices by JAX's collectives and lax.ppermute only.
A program may use at most 128 MiB of HBM per device.

v0:
```python
from functools import partial

import jax
import jax.numpy as jnp
from jax import lax
from jax.experimental import pallas as pl
from jax.experimental.pallas import tpu as pltpu
from jax.sharding import Mesh, PartitionSpec as P


NEG_FILL = -1e30
HEAD_SCALE = 0.8
NZ, NX, NY, NC = 8, 4, 4, 2
TOK = 256
D = 2048
HALF = 128
CAP = 8
SLOTS = NZ * NX * CAP
LOG2E = 1.4426950408889634
BF = jnp.bfloat16
F32 = jnp.float32
SMEM = pl.BlockSpec(memory_space=pltpu.SMEM)
VMEM = pl.BlockSpec(memory_space=pltpu.VMEM)
VLIM = 28 * 1024 * 1024


def shift(value, axis, step):
    size = lax.axis_size(axis)
    return lax.ppermute(value, axis, [(i, (i + step) % size) for i in range(size)])


def swap(value):
    return shift(value, "c", 1)


def after(value, *others):
    return lax.optimization_barrier((value, *others))[0]


def call(kernel, scalars, operands, outs, scratch=(), flops=0):
    return pl.pallas_call(
        kernel,
        out_shape=outs,
        in_specs=[SMEM] * len(scalars) + [VMEM] * len(operands),
        out_specs=jax.tree.map(lambda _: VMEM, outs),
        scratch_shapes=list(scratch),
        compiler_params=pltpu.CompilerParams(vmem_limit_bytes=VLIM),
        cost_estimate=pl.CostEstimate(flops=flops, bytes_accessed=0, transcendentals=0),
    )(*scalars, *operands)


def iota(shape, dim):
    return lax.broadcasted_iota(jnp.int32, shape, dim)


LINES = HALF + 8


def pack_kernel(pos, lam, docs, q1, q2, k1, k2, v, *rest):
    outs, (q1v, q2v, k1v, k2v, vv, sems) = rest[:4], rest[4:]
    pairs = ((q1, q1v), (q2, q2v), (k1, k1v), (k2, k2v), (v, vv))
    loads = [pltpu.make_async_copy(a, b, sems.at[i]) for i, (a, b) in enumerate(pairs)]
    for load in loads:
        load.start()
    x = pos[1]
    row = iota((128, 128), 0)
    col = iota((128, 128), 1)
    place = iota((TOK, 128), 0)
    lane = iota((TOK, 128), 1)
    line = iota((8, 128), 0)
    numbers = jnp.broadcast_to(docs[...].astype(F32), (8, TOK)).astype(BF)
    for load in loads:
        load.wait()
    for turn, out in enumerate(outs):
        index = x ^ turn
        head = index >> 1
        core = index & 1
        first = ((col < 64) & (row == col + 64 * head)).astype(BF)
        second = ((col >= 64) & (row == col - 64 + 64 * head)).astype(BF)

        def rows(ref, lanes):
            return jnp.concatenate(
                [
                    ref[pl.ds(pl.multiple_of(64 * i + 32 * core, 32), 32), lanes]
                    for i in range(4)
                ],
                axis=0,
            )

        every = slice(None)

        def merged(a, b):
            return (
                jnp.dot(rows(a, every), first, preferred_element_type=F32)
                + jnp.dot(rows(b, every), second, preferred_element_type=F32)
            ).astype(BF)

        out[0:HALF, 0:128] = merged(q1v, q2v)
        out[0:HALF, 128:256] = merged(k1v, k2v)
        out[0:HALF, 256:384] = rows(vv, pl.ds(pl.multiple_of(128 * head, 128), 128))
        taken = (place == 64 * (lane >> 5) + 32 * core + (lane & 31)).astype(BF)
        own_docs = jnp.dot(numbers, taken, preferred_element_type=F32)
        mixing = jnp.where(head == 0, lam[0], lam[1])
        mixing = jnp.full((8, 128), mixing, F32)
        upper = mixing.astype(BF).astype(F32)
        middle = (mixing - upper).astype(BF).astype(F32)
        lower = mixing - upper - middle
        extra = jnp.where(
            line == 0,
            own_docs,
            jnp.where(line == 1, upper, jnp.where(line == 2, middle, lower)),
        ).astype(BF)
        out[HALF:LINES, 0:128] = extra
        out[HALF:LINES, 128:256] = extra
        out[HALF:LINES, 256:384] = extra


def unpack_kernel(pos, r0, r1, r2, r3, keys, edge, queries, docs, lam):
    mine = (pos[1] & 1) * 2 + pos[3]
    lane = iota((HALF, 128), 1)
    unit = (iota((HALF, 128), 0) == lane).astype(BF)
    for turn, ref in enumerate((r0, r1, r2, r3)):
        block = mine ^ turn
        keys[block] = ref[:, 128:384]

        @pl.when(block == NX - 1)
        def _():
            edge[...] = ref[:, 128:384]

        both = ref[0:HALF, 0:128]
        start = pl.multiple_of(block * HALF, HALF)
        queries[pl.ds(start, HALF), :] = jnp.where(lane < 64, both, jnp.zeros_like(both))
        queries[pl.ds(start + 512, HALF), :] = jnp.where(lane < 64, jnp.zeros_like(both), both)
        extra = ref[HALF:LINES, 0:128].astype(F32)
        spread = jnp.broadcast_to(extra[0:1, :], (HALF, 128)).astype(BF)
        column = lax.dot_general(
            unit, spread, (((1,), (1,)), ((), ())), preferred_element_type=F32
        )
        docs[pl.ds(start, HALF), :] = column
        docs[pl.ds(start + 512, HALF), :] = column
        if turn == 0:
            total = extra[1:2, :] + extra[2:3, :] + extra[3:4, :]
            lam[...] = jnp.broadcast_to(total, (8, 128))


ROWS = 256


def attend_kernel(kinds, first_call, last_call, pos, *refs):
    refs = list(refs)
    queries, query_docs = refs[0], refs[1]
    at = 2
    if last_call:
        lam, gain = refs[at], refs[at + 1]
        at += 2
    if not first_call:
        state_in = refs[at : at + 3]
        at += 3
    planes = []
    for back, blocks in kinds:
        count = 2
        planes.append((back, blocks, refs[at : at + count]))
        at += count
    if last_call:
        out = refs[at]
        tops, sums, acc = refs[at + 1 : at + 4]
    else:
        tops, sums, acc = refs[at : at + 3]
    z, core = pos[0], pos[3]
    least = jnp.min(query_docs[0:8, :])

    def setup(tile):
        rows = pl.ds(pl.multiple_of(tile * ROWS, ROWS), ROWS)
        if first_call:
            tops[rows, :] = jnp.full((ROWS, 128), NEG_FILL, F32)
            sums[rows, :] = jnp.zeros((ROWS, 128), F32)
            acc[rows, :] = jnp.zeros((ROWS, 128), F32)
        else:
            for dst, src in zip((tops, sums, acc), state_in):
                dst[rows, :] = src[rows, :]

    def step(tile, back, blocks, arrays):
        rows = pl.ds(pl.multiple_of(tile * ROWS, ROWS), ROWS)
        count = blocks * TOK
        parts = [
            ref[:, :] if blocks == 1 else ref[b] for b in range(blocks) for ref in arrays
        ]
        numbers = jnp.concatenate([p[HALF:LINES, 0:128].astype(F32) for p in parts], axis=1)
        key_docs = numbers[0:1, :]
        parts = [p[0:HALF] for p in parts]
        keys = jnp.concatenate([p[:, 0:128] for p in parts], axis=0)
        vals = jnp.concatenate([p[:, 128:256] for p in parts], axis=0)
        raw = lax.dot_general(
            queries[rows, :], keys, (((1,), (1,)), ((), ())), preferred_element_type=F32
        )
        scaled = raw * (0.125 * LOG2E)
        allowed = key_docs == query_docs[rows, :][:, 0:1]
        if back == 0:
            at_key = iota((1, count), 1)
            lane = at_key & 127
            key_pos = (
                (at_key >> 8) * TOK
                + 64 * (lane >> 5)
                + 32 * (core ^ ((at_key >> 7) & 1))
                + (lane & 31)
            )
            at_row = (iota((ROWS, 1), 0) + tile * ROWS) & 511
            row = at_row & 127
            query_pos = (at_row >> 7) * TOK + 64 * (row >> 5) + 32 * core + (row & 31)
            allowed = allowed & (key_pos <= query_pos)
        masked = jnp.where(allowed, scaled, NEG_FILL)
        old = tops[rows, :][:, 0:1]
        new = jnp.maximum(old, jnp.max(masked, axis=1, keepdims=True))
        probs = jnp.exp2(masked - new)
        fade = jnp.exp2(old - new)
        tops[rows, :] = jnp.broadcast_to(new, (ROWS, 128))
        sums[rows, :] = sums[rows, :] * fade + jnp.sum(probs, axis=1, keepdims=True)
        acc[rows, :] = acc[rows, :] * fade + jnp.dot(
            probs.astype(BF), vals, preferred_element_type=F32
        )

    def over_tiles(body):
        def turn(tile, carry):
            body(tile)
            return carry

        lax.fori_loop(0, 1024 // ROWS, turn, 0)

    over_tiles(setup)
    for back, blocks, arrays in planes:
        if back == 0:
            over_tiles(lambda tile: step(tile, back, blocks, arrays))
        else:

            last = [ref[...] if blocks == 1 else ref[3] for ref in arrays]
            latest = jnp.max(jnp.maximum(*[p[HALF : HALF + 1, 0:128].astype(F32) for p in last]))

            @pl.when((z >= back) & (latest >= least))
            def _():
                over_tiles(lambda tile: step(tile, back, blocks, arrays))

    if last_call:
        one = acc[0:512, :] / sums[0:512, :]
        two = acc[512:1024, :] / sums[512:1024, :]
        head = one - lam[0:1, :] * two
        scale = lax.rsqrt(jnp.mean(head * head, axis=1, keepdims=True) + 1e-5)
        out[...] = (head * scale * gain[...] * HEAD_SCALE).astype(BF)


def attend(pos, queries, docs, planes, state=None, finish=None):
    kinds = tuple((back, blocks) for back, blocks, _ in planes)
    operands = [queries, docs]
    if finish is not None:
        operands += list(finish)
    if state is not None:
        operands += list(state)
    for _, _, arrays in planes:
        operands += list(arrays)
    big = jax.ShapeDtypeStruct((1024, 128), F32)
    kernel = partial(attend_kernel, kinds, state is None, finish is not None)
    keys = sum(blocks * TOK for _, blocks in kinds)
    if finish is not None:
        outs = jax.ShapeDtypeStruct((512, 128), BF)
        scratch = [pltpu.VMEM((1024, 128), F32)] * 3
    else:
        outs = (big, big, big)
        scratch = []
    return call(kernel, [pos], operands, outs, scratch, flops=1024 * keys * 512)


def project_kernel(pos, attn, resid, gain, *refs):
    weights, (mixed, normed) = refs[:-2], refs[-2:]
    y, core = pos[2], pos[3]
    total = resid[...].astype(F32)
    order = []
    for flip in range(2):
        for ahead, w in zip((0, 3, 1, 2), weights[4 * flip : 4 * flip + 4]):
            order.append((w, ahead, flip))
    for w, ahead, flip in order:
        src = (y + ahead) & 3
        head = 2 * (core ^ flip)
        lhs = jnp.concatenate([attn[head * 4 + src], attn[(head + 1) * 4 + src]], axis=1)
        total = total + jnp.dot(lhs, w[...], preferred_element_type=F32)
    mixed[...] = total
    scale = lax.rsqrt(jnp.mean(total * total, axis=1, keepdims=True) + 1e-6)
    normed[...] = (total * scale * gain[...]).astype(BF)


def route_kernel(pos, routes, weights, pick, high, low):
    core = pos[3]
    group = pos[2] * NC + core
    at = iota((TOK, TOK), 1)
    token = ((at >> 5) & 3) * 64 + 32 * (core ^ (at >> 7)) + (at & 31)
    order = (iota((TOK, TOK), 0) == token).astype(F32)

    def arranged(table):
        return lax.dot_general(
            table,
            order,
            (((0,), (0,)), ((), ())),
            preferred_element_type=F32,
            precision=lax.Precision.HIGHEST,
        )

    ids = arranged(routes[...].astype(F32)).astype(jnp.int32)
    gain = arranged(weights[...])
    target = iota((NZ * NX, TOK), 0) * (NY * NC) + group
    hits = jnp.zeros((NZ * NX, TOK), F32)
    gains = jnp.zeros((NZ * NX, TOK), F32)
    for k in range(4):
        same = ids[k : k + 1, :] == target
        hits = hits + jnp.where(same, 1.0, 0.0)
        gains = gains + jnp.where(same, gain[k : k + 1, :], 0.0)
    before = (iota((TOK, TOK), 0) < iota((TOK, TOK), 1)).astype(BF)
    rank = jnp.dot(hits.astype(BF), before, preferred_element_type=F32)
    rank = jnp.where(hits > 0.5, rank, -1.0)
    slot = iota((NZ * NX, CAP, TOK), 1).astype(F32)
    chosen = (jnp.broadcast_to(rank[:, None, :], (NZ * NX, CAP, TOK)) == slot).reshape(SLOTS, TOK)
    spread = jnp.broadcast_to(gains[:, None, :], (NZ * NX, CAP, TOK)).reshape(SLOTS, TOK)
    pick[...] = jnp.where(chosen, 1.0, 0.0).astype(BF)
    full = jnp.where(chosen, spread, 0.0).T
    upper = full.astype(BF)
    high[...] = upper
    low[...] = (full - upper.astype(F32)).astype(BF)


def dispatch_kernel(pos, pick, *refs):
    chunks, (outgoing, rows) = refs[:-2], refs[-2:]
    y = pos[2]
    for flip in range(2):
        for ahead, ref in zip((0, 3, 1, 2), chunks[4 * flip : 4 * flip + 4]):
            src = (y + ahead) & 3
            rows[pl.ds(pl.multiple_of(flip * HALF + src * 32, 32), 32), :] = ref[...]
    outgoing[...] = jnp.dot(pick[...], rows[...], preferred_element_type=F32).astype(BF)


def shared_kernel(rows, gate, up, down, out):
    gated = jnp.dot(rows[...], gate[...], preferred_element_type=F32)
    lifted = jnp.dot(rows[...], up[...], preferred_element_type=F32)
    act = (gated / (1.0 + jnp.exp(-gated)) * lifted).astype(BF)
    out[...] = jnp.dot(act, down[...], preferred_element_type=F32)


def expert_kernel(rows, gate, up, down, out, acc):
    step = pl.program_id(0)
    gated = jnp.dot(rows[...], gate[0], preferred_element_type=F32)
    lifted = jnp.dot(rows[...], up[0], preferred_element_type=F32)
    act = (gated / (1.0 + jnp.exp(-gated)) * lifted).astype(BF)
    piece = jnp.dot(act, down[0], preferred_element_type=F32)

    @pl.when(step == 0)
    def _():
        acc[...] = piece

    @pl.when(step == 1)
    def _():
        out[...] = (acc[...] + piece).astype(BF)


def experts(rows, gate, up, down):
    width = gate.shape[2] // 2
    whole = pl.BlockSpec((SLOTS, D), lambda i: (0, 0))
    return pl.pallas_call(
        expert_kernel,
        grid=(2,),
        out_shape=jax.ShapeDtypeStruct((SLOTS, D), BF),
        in_specs=[
            whole,
            pl.BlockSpec((1, D, width), lambda i: (0, 0, i)),
            pl.BlockSpec((1, D, width), lambda i: (0, 0, i)),
            pl.BlockSpec((1, width, D), lambda i: (0, i, 0)),
        ],
        out_specs=whole,
        scratch_shapes=[pltpu.VMEM((SLOTS, D), F32)],
        compiler_params=pltpu.CompilerParams(vmem_limit_bytes=VLIM),
        cost_estimate=pl.CostEstimate(
            flops=2 * SLOTS * D * 1536, bytes_accessed=0, transcendentals=0
        ),
        name="expert",
    )(rows, gate, up, down)


def combine_kernel(high, low, rows, shared, keep, send):
    total = (
        jnp.dot(high[...], rows[...], preferred_element_type=F32)
        + jnp.dot(low[...], rows[...], preferred_element_type=F32)
        + shared[...]
    ).astype(BF)
    keep[...] = total[:HALF]
    send[...] = total[HALF:]


def layer(
    resid,
    query_one,
    query_two,
    key_one,
    key_two,
    values,
    documents,
    mix_lambda,
    head_gain,
    out_weight,
    ffn_gain,
    routes,
    route_weight,
    expert_gate,
    expert_up,
    expert_down,
    shared_gate,
    shared_up,
    shared_down,
):
    iz, ix, iy, ic = (lax.axis_index(a) for a in ("z", "x", "y", "c"))
    pos = jnp.stack([iz, ix, iy, ic, jnp.int32(0)])
    plane_axes = ("z", "x")

    any_space = pl.BlockSpec(memory_space=pltpu.HBM)
    packed = pl.pallas_call(
        pack_kernel,
        out_shape=tuple(jax.ShapeDtypeStruct((LINES, 384), BF) for _ in range(4)),
        in_specs=[SMEM, SMEM, VMEM] + [any_space] * 5,
        out_specs=(VMEM,) * 4,
        scratch_shapes=[pltpu.VMEM((TOK, HALF), BF)] * 4
        + [pltpu.VMEM((TOK, 256), BF), pltpu.SemaphoreType.DMA((5,))],
        compiler_params=pltpu.CompilerParams(vmem_limit_bytes=62 * 1024 * 1024),
        name="pack",
    )(pos, mix_lambda, documents.reshape(1, TOK), query_one, query_two, key_one, key_two, values)

    def turn_pairs(turn):
        pairs = []
        for x in range(NX):
            for c in range(NC):
                index = x ^ turn
                pairs.append((x * NC + c, (2 * c + (index >> 1)) * NC + (index & 1)))
        return pairs

    came = [lax.ppermute(packed[t], ("x", "c"), turn_pairs(t)) for t in range(4)]
    keys0, edge, queries, docs, lam = call(
        unpack_kernel,
        [pos],
        came,
        (
            jax.ShapeDtypeStruct((NX, LINES, 256), BF),
            jax.ShapeDtypeStruct((LINES, 256), BF),
            jax.ShapeDtypeStruct((1024, 128), BF),
            jax.ShapeDtypeStruct((1024, 128), F32),
            jax.ShapeDtypeStruct((8, 128), F32),
        ),
    )
    table = jax.ShapeDtypeStruct((SLOTS, TOK), BF)
    pick, weight_high, weight_low = call(
        route_kernel, [pos], [routes, route_weight], (table, table, table)
    )

    queries = after(queries, pick, weight_high, weight_low)
    keys1 = shift(keys0, "z", 1)
    back3 = shift(edge, "z", -3)
    state = attend(pos, queries, docs, [(0, 4, [keys0, swap(keys0)])])
    keys2 = shift(keys1, "z", 1)
    state = attend(pos, queries, docs, [(1, 4, [keys1, swap(keys1)])], state)
    keys3 = shift(keys2, "z", 1)
    pair5 = [back3, swap(back3)]
    state = attend(pos, queries, docs, [(2, 4, [keys2, swap(keys2)]), (5, 1, pair5)], state)
    keys4 = shift(keys3, "z", 1)
    state = attend(pos, queries, docs, [(3, 4, [keys3, swap(keys3)])], state)
    heads = attend(
        pos,
        queries,
        docs,
        [(4, 4, [keys4, swap(keys4)])],
        state,
        finish=(lam, head_gain.reshape(1, 128)),
    )

    held = after(out_weight, packed[0])
    mine = [out_weight] + [shift(held, "y", k) for k in (1, -1, 2)]
    full_weight = mine + [swap(after(w, heads)) for w in mine]

    attn = lax.all_to_all(
        heads.reshape(NX * NY, 32, 128), ("x", "y"), split_axis=0, concat_axis=0, tiled=True
    )
    own_start = (iy * NC + ic) * 32
    resid_own = lax.dynamic_slice_in_dim(resid, own_start, 32, 0)
    mixed, normed = call(
        project_kernel,
        [pos],
        [attn, resid_own, ffn_gain.reshape(1, D)] + full_weight,
        (
            jax.ShapeDtypeStruct((32, D), F32),
            jax.ShapeDtypeStruct((32, D), BF),
        ),
        flops=2 * 32 * D * D,
    )

    chunks = [normed] + [shift(normed, "y", k) for k in (1, -1, 2)]
    chunks = chunks + [swap(c) for c in chunks]
    outgoing, rows = call(
        dispatch_kernel,
        [pos],
        [pick] + chunks,
        (jax.ShapeDtypeStruct((SLOTS, D), BF), jax.ShapeDtypeStruct((TOK, D), BF)),
        flops=2 * SLOTS * TOK * D,
    )
    arrived = lax.all_to_all(
        outgoing.reshape(NZ * NX, CAP, D), plane_axes, split_axis=0, concat_axis=0, tiled=True
    )
    shared = call(
        shared_kernel,
        [],
        [rows, shared_gate, shared_up, shared_down],
        jax.ShapeDtypeStruct((TOK, D), F32),
        flops=2 * TOK * D * 192,
    )
    result = experts(arrived.reshape(SLOTS, D), expert_gate, expert_up, expert_down)
    returned = lax.all_to_all(
        result.reshape(NZ * NX, CAP, D), plane_axes, split_axis=0, concat_axis=0, tiled=True
    ).reshape(SLOTS, D)
    part = jax.ShapeDtypeStruct((HALF, D), BF)
    keep, send = call(
        combine_kernel,
        [],
        [weight_high, weight_low, returned, shared],
        (part, part),
        flops=4 * SLOTS * TOK * D,
    )
    pair_sum = (keep.astype(F32) + swap(send).astype(F32)).astype(BF)
    ffn = lax.all_to_all(
        pair_sum.reshape(NY, 32, D), "y", split_axis=0, concat_axis=0, tiled=True
    )
    return (mixed + ffn.astype(F32).sum(axis=0)).astype(BF)


def solution(mesh):
    split = Mesh(mesh.devices.reshape(NZ, NX, NY, NC), ("z", "x", "y", "c"))
    sp, tp, both = ("z", "x"), ("y", "c"), ("z", "x", "y", "c")
    placed = (
        P(sp, None),
        P(sp, tp),
        P(sp, tp),
        P(sp, tp),
        P(sp, tp),
        P(sp, tp),
        P(sp),
        P(tp),
        P(),
        P(tp, None),
        P(),
        P(sp, None),
        P(sp, None),
        P(both, None, None),
        P(both, None, None),
        P(both, None, None),
        P(None, tp),
        P(None, tp),
        P(tp, None),
    )
    return jax.shard_map(
        layer, mesh=split, in_specs=placed, out_specs=P(both, None), check_vma=False
    )
```

profile of v0, /device:TPU:2, one launch (start us, length us, event | category | flops | bytes accessed | tf_op | source)
XLA Modules:
  0.0 212.4 jit_solution(12484480915443563756)
XLA Ops:
  0.6 2.7 %pack.1 = (bf16[136,384]{1,0:T(8,128)(2,1)}, bf16[136,384]{1,0:T(8,128)(2,1)}, bf16[136,384]{1,0:T(8,128)(2,1)}, bf16[136,384]{1,0:T(8,128)(2,1)}) custom-call(s32[5]{0:T(128)} %stack.19.pos, f32[2]{0:T(128)} %lam.1, s32[1,256]{1,0:T(1,128)} %bitcast.20, bf16[256,128]{1,0:T(8,128)(2,1)} %q1.1, bf16[256,128]{1,0:T(8,128)(2,1)} %q2.1, bf16[256,128]{1,0:T(8,128)(2,1)} %k1.1, ...), custom_call_target="tpu_custom_call" | custom-call | tf_op jit(solution)/shard_map/pack/pallas_call | solution.py:419
  3.3 1.9 collective-permute-start
  5.3 1.9 collective-permute-start.1
  7.5 1.5 collective-permute-start.3
  9.0 1.8 collective-permute-done.r0
  10.8 2.5 %collective-permute-done.1.r1 = bf16[136,384]{1,0:T(8,128)(2,1)S(1)} collective-permute-done((bf16[136,384]{1,0:T(8,128)(2,1)}, bf16[136,384]{1,0:T(8,128)(2,1)S(1)}, u32[]{:S(2)}, u32[]{:S(2)}) %collective-permute-start.1) | collective-permute-done | bytes 104480 | tf_op jit(solution)/shard_map/ppermute | solution.py:438
  13.9 1.2 shard_map.181
  15.1 2.0 collective-permute-start.5
  17.1 2.0 collective-permute-start.4
  19.8 5.8 %collective-permute-start.9 = (bf16[136,256]{1,0:T(8,128)(2,1)S(1)}, bf16[136,256]{1,0:T(8,128)(2,1)S(1)}, u32[]{:S(2)}, u32[]{:S(2)}) collective-permute-start(bf16[136,256]{1,0:T(8,128)(2,1)S(1)} %get-tuple-element.59), channel_id=1, source_target_pairs={{0,160},{32,192},{64,224},{96,0},{128,32},{160,64},{192,96},{224,1... | collective-permute-start | bytes 208904 | tf_op jit(solution)/shard_map/ppermute | solution.py:29
  25.7 1.3 collective-permute-done.5.refs_5_
  27.0 4.1 %collective-permute-done.9.refs_7_ = bf16[136,256]{1,0:T(8,128)(2,1)S(1)} collective-permute-done((bf16[136,256]{1,0:T(8,128)(2,1)S(1)}, bf16[136,256]{1,0:T(8,128)(2,1)S(1)}, u32[]{:S(2)}, u32[]{:S(2)}) %collective-permute-start.9) | collective-permute-done | bytes 69664 | tf_op jit(solution)/shard_map/ppermute | solution.py:29
  31.6 1.6 collective-permute-start.15
  33.2 1.7 collective-permute-start.16
  35.5 2.0 collective-permute-start.17
  38.2 1.5 collective-permute-done.6.refs_6_
  39.9 8.6 %collective-permute-done.11.refs_5_ = bf16[4,136,256]{2,1,0:T(8,128)(2,1)S(1)} collective-permute-done((bf16[4,136,256]{2,1,0:T(8,128)(2,1)S(1)}, bf16[4,136,256]{2,1,0:T(8,128)(2,1)S(1)}, u32[]{:S(2)}, u32[]{:S(2)}) %collective-permute-start.11) | collective-permute-done | bytes 278560 | tf_op jit(solution)/shard_map/ppermute | solution.py:29
  48.5 9.6 %collective-permute-done.13.refs_7_ = bf16[4,136,256]{2,1,0:T(8,128)(2,1)} collective-permute-done((bf16[4,136,256]{2,1,0:T(8,128)(2,1)S(1)}, bf16[4,136,256]{2,1,0:T(8,128)(2,1)}, u32[]{:S(2)}, u32[]{:S(2)}) %collective-permute-start.13) | collective-permute-done | bytes 278560 | tf_op jit(solution)/shard_map/ppermute | solution.py:29
  60.4 1.1 shard_map.182
  64.1 1.0 copy-done.30
  65.1 1.0 copy-done.32
  66.0 4.2 %shard_map.183 = (f32[1024,128]{1,0:T(8,128)S(1)}, f32[1024,128]{1,0:T(8,128)S(1)}, f32[1024,128]{1,0:T(8,128)S(1)}) custom-call(s32[5]{0:T(128)S(1)} %copy-done.25, bf16[1024,128]{1,0:T(8,128)(2,1)S(1)} %get-tuple-element.49.refs_0_, f32[1024,128]{1,0:T(8,128)S(1)} %get-tuple-element.50.refs_1_, bf16[4,136,256]{2,1,0:T(8,128)(2,1)S(1)} %copy-done.30, ...), custom_call_target="tpu_custom_call" | custom-call | flops 536870912 | tf_op jit(solution)/shard_map/pallas_call | solution.py:41
  70.2 0.9 shard_map.184
  71.1 1.0 shard_map.185
  72.2 1.3 shard_map.186
  73.6 2.3 %shard_map.187 = bf16[512,128]{1,0:T(8,128)(2,1)} custom-call(s32[5]{0:T(128)S(1)} %copy-done.25, bf16[1024,128]{1,0:T(8,128)(2,1)S(1)} %get-tuple-element.49.refs_0_, f32[1024,128]{1,0:T(8,128)S(1)} %get-tuple-element.50.refs_1_, f32[8,128]{1,0:T(8,128)S(1)} %get-tuple-element.51.refs_2_, f32[1,128]{1,0:T(1,128)S(1)} %bitcast.18, ...), custom_call_target="tpu_custom_call" | custom-call | flops 536870912 | tf_op jit(solution)/shard_map/pallas_call | solution.py:41
  76.5 6.0 %collective-permute-done.17.refs_3_ = bf16[256,2048]{1,0:T(8,128)(2,1)} collective-permute-done((bf16[256,2048]{1,0:T(8,128)(2,1)}, bf16[256,2048]{1,0:T(8,128)(2,1)}, u32[]{:S(2)}, u32[]{:S(2)}) %collective-permute-start.17) | collective-permute-done | bytes 1048608 | tf_op jit(solution)/shard_map/ppermute | solution.py:29
  83.0 8.3 %all-to-all-start = ((bf16[16,32,128]{2,1,0:T(8,128)(2,1)}), bf16[16,32,128]{2,1,0:T(8,128)(2,1)S(1)}, u32[]{:S(2)}, u32[]{:S(2)}) async-start(bf16[16,32,128]{2,1,0:T(8,128)(2,1)} %bitcast.6), calls=%async_computation | async-start | bytes 262144 | tf_op jit(solution)/shard_map/all_to_all | solution.py:480
  91.3 6.4 %all-to-all-done.attn = bf16[16,32,128]{2,1,0:T(8,128)(2,1)S(1)} async-done(((bf16[16,32,128]{2,1,0:T(8,128)(2,1)}), bf16[16,32,128]{2,1,0:T(8,128)(2,1)S(1)}, u32[]{:S(2)}, u32[]{:S(2)}) %all-to-all-start) | async-done | bytes 131104 | tf_op jit(solution)/shard_map/all_to_all | solution.py:480
  97.7 4.9 %shard_map.188 = (f32[32,2048]{1,0:T(8,128)S(1)}, bf16[32,2048]{1,0:T(8,128)(2,1)S(1)}) custom-call(s32[5]{0:T(128)S(1)} %copy-done.26, bf16[16,32,128]{2,1,0:T(8,128)(2,1)S(1)} %all-to-all-done.attn, bf16[32,2048]{1,0:T(8,128)(2,1)S(1)} %constant_dynamic-slice_fusion.resid, f32[1,2048]{1,0:T(1,128)S(1)} %bitcast.17, bf16[256,2048]{1,0:T(8,128)(2,1)S(1)} %copy-done.7, ...), custom_call_target="tpu_custom_call" | custom-call | flops 268435456 | tf_op jit(solution)/shard_map/pallas_call | solution.py:41
  103.8 2.8 %collective-permute-start.23 = (bf16[32,2048]{1,0:T(8,128)(2,1)S(1)}, bf16[32,2048]{1,0:T(8,128)(2,1)S(1)}, u32[]{:S(2)}, u32[]{:S(2)}) collective-permute-start(bf16[32,2048]{1,0:T(8,128)(2,1)S(1)} %get-tuple-element.72.refs_0_), channel_id=1, source_target_pairs={{0,6},{2,0},{4,2},{6,4},{1,7},{3,1},{5,3},{7,5},{8,14},{10,8},{12,... | collective-permute-start | bytes 393224 | tf_op jit(solution)/shard_map/ppermute | solution.py:29
  106.9 4.0 %collective-permute-done.22.refs_1_ = bf16[32,2048]{1,0:T(8,128)(2,1)S(1)} collective-permute-done((bf16[32,2048]{1,0:T(8,128)(2,1)S(1)}, bf16[32,2048]{1,0:T(8,128)(2,1)S(1)}, u32[]{:S(2)}, u32[]{:S(2)}) %collective-permute-start.22) | collective-permute-done | bytes 131104 | tf_op jit(solution)/shard_map/ppermute | solution.py:29
  111.5 1.6 collective-permute-done.24.refs_3_
  113.1 1.3 collective-permute-done.28.refs_7_
  114.4 1.1 shard_map.189
  115.5 40.8 %all_to_all.20 = bf16[32,8,2048]{2,1,0:T(8,128)(2,1)S(1)} all-to-all(bf16[32,8,2048]{2,1,0:T(8,128)(2,1)S(1)} %bitcast.16), channel_id=1, replica_groups=mesh['z'=8,'x'=4,'y'=4,'c'=2] {'z','x'}, dimensions={0} | all-to-all | bytes 2097152 | tf_op jit(solution)/shard_map/all_to_all | solution.py:505
  156.3 2.8 %expert.1 = bf16[256,2048]{1,0:T(8,128)(2,1)S(1)} custom-call(bf16[256,2048]{1,0:T(8,128)(2,1)S(1)} %bitcast.15, bf16[1,2048,512]{2,1,0:T(8,128)(2,1)S(1)} %copy-done.4, bf16[1,2048,512]{2,1,0:T(8,128)(2,1)S(1)} %copy-done.5, bf16[1,512,2048]{2,1,0:T(8,128)(2,1)S(1)} %copy-done.6), custom_call_target="tpu_custom_call" | custom-call | flops 1610612736 | tf_op jit(solution)/shard_map/expert/pallas_call | solution.py:363
  159.2 1.0 copy-done.3
  160.2 5.7 %all-to-all-start.2 = ((bf16[32,8,2048]{2,1,0:T(8,128)(2,1)}), bf16[32,8,2048]{2,1,0:T(8,128)(2,1)S(1)}, u32[]{:S(2)}, u32[]{:S(2)}) async-start(bf16[32,8,2048]{2,1,0:T(8,128)(2,1)} %bitcast.14), calls=%async_computation.2 | async-start | bytes 2097152 | tf_op jit(solution)/shard_map/all_to_all | solution.py:516
  166.2 1.2 copy.23.up
  167.4 1.2 copy-done.9
  168.6 1.0 shard_map.190.shared
  169.7 1.3 copy-done.1
  171.0 22.0 %all-to-all-done.2 = bf16[32,8,2048]{2,1,0:T(8,128)(2,1)S(1)} async-done(((bf16[32,8,2048]{2,1,0:T(8,128)(2,1)}), bf16[32,8,2048]{2,1,0:T(8,128)(2,1)S(1)}, u32[]{:S(2)}, u32[]{:S(2)}) %all-to-all-start.2) | async-done | bytes 1048608 | tf_op jit(solution)/shard_map/all_to_all | solution.py:516
  193.0 1.6 copy-done.2
  194.6 0.9 copy-done.18
  196.3 1.9 collective-permute-done.29
  198.3 13.2 %all_to_all.21 = bf16[4,32,2048]{2,1,0:T(8,128)(2,1)S(1)} all-to-all(bf16[4,32,2048]{2,1,0:T(8,128)(2,1)S(1)} %bitcast.19), channel_id=1, replica_groups=mesh['z'=8,'x'=4,'y'=4,'c'=2] {'y'}, dimensions={0} | all-to-all | bytes 1048576 | tf_op jit(solution)/shard_map/all_to_all | solution.py:528
  (108 shorter events, 14.4 us)
Async XLA Ops:
  0.0 91.3 %copy-start = (bf16[256,2048]{1,0:T(8,128)(2,1)S(1)}, bf16[256,2048]{1,0:T(8,128)(2,1)}, u32[]{:S(2)}) copy-start(bf16[256,2048]{1,0:T(8,128)(2,1)} %param.19) | copy-start | bytes 3145732
  3.3 7.5 %collective-permute-start = (bf16[136,384]{1,0:T(8,128)(2,1)}, bf16[136,384]{1,0:T(8,128)(2,1)S(1)}, u32[]{:S(2)}, u32[]{:S(2)}) collective-permute-start(bf16[136,384]{1,0:T(8,128)(2,1)} %get-tuple-element.41), channel_id=1, source_target_pairs={{0,0},{1,16},{8,1},{9,17},{16,8},{17,24},{24,9},{25,25},{2,2},{3,1... | collective-permute-start | bytes 313352 | tf_op jit(solution)/shard_map/ppermute | solution.py:438
  5.3 8.0 %collective-permute-start.1 = (bf16[136,384]{1,0:T(8,128)(2,1)}, bf16[136,384]{1,0:T(8,128)(2,1)S(1)}, u32[]{:S(2)}, u32[]{:S(2)}) collective-permute-start(bf16[136,384]{1,0:T(8,128)(2,1)} %get-tuple-element.42), channel_id=1, source_target_pairs={{0,1},{1,17},{8,0},{9,16},{16,9},{17,25},{24,8},{25,24},{2,3},{3,1... | collective-permute-start | bytes 313352 | tf_op jit(solution)/shard_map/ppermute | solution.py:438
  7.1 6.2 %collective-permute-start.2 = (bf16[136,384]{1,0:T(8,128)(2,1)}, bf16[136,384]{1,0:T(8,128)(2,1)S(1)}, u32[]{:S(2)}, u32[]{:S(2)}) collective-permute-start(bf16[136,384]{1,0:T(8,128)(2,1)} %get-tuple-element.43), channel_id=1, source_target_pairs={{0,8},{1,24},{8,9},{9,25},{16,0},{17,16},{24,1},{25,17},{2,10},{3,... | collective-permute-start | bytes 313352 | tf_op jit(solution)/shard_map/ppermute | solution.py:438
  7.5 5.8 %collective-permute-start.3 = (bf16[136,384]{1,0:T(8,128)(2,1)}, bf16[136,384]{1,0:T(8,128)(2,1)S(1)}, u32[]{:S(2)}, u32[]{:S(2)}) collective-permute-start(bf16[136,384]{1,0:T(8,128)(2,1)} %get-tuple-element.44), channel_id=1, source_target_pairs={{0,9},{1,25},{8,8},{9,24},{16,1},{17,17},{24,0},{25,16},{2,11},{3,... | collective-permute-start | bytes 313352 | tf_op jit(solution)/shard_map/ppermute | solution.py:438
  15.1 11.8 %collective-permute-start.5 = (bf16[4,136,256]{2,1,0:T(8,128)(2,1)S(1)}, bf16[4,136,256]{2,1,0:T(8,128)(2,1)S(1)}, u32[]{:S(2)}, u32[]{:S(2)}) collective-permute-start(bf16[4,136,256]{2,1,0:T(8,128)(2,1)S(1)} %get-tuple-element.52.refs_2_), channel_id=1, source_target_pairs={{0,32},{32,64},{64,96},{96,128},{128,160},{160,192},{192,224},{224... | collective-permute-start | bytes 835592 | tf_op jit(solution)/shard_map/ppermute | solution.py:29
  17.1 20.4 %collective-permute-start.4 = (bf16[4,136,256]{2,1,0:T(8,128)(2,1)S(1)}, bf16[4,136,256]{2,1,0:T(8,128)(2,1)S(1)}, u32[]{:S(2)}, u32[]{:S(2)}) collective-permute-start(bf16[4,136,256]{2,1,0:T(8,128)(2,1)S(1)} %get-tuple-element.52.refs_2_), channel_id=1, source_target_pairs={{0,1},{1,0},{2,3},{3,2},{4,5},{5,4},{6,7},{7,6},{8,9},{9,8},{10,11... | collective-permute-start | bytes 835592 | tf_op jit(solution)/shard_map/ppermute | solution.py:29
  19.8 11.2 %collective-permute-start.9 = (bf16[136,256]{1,0:T(8,128)(2,1)S(1)}, bf16[136,256]{1,0:T(8,128)(2,1)S(1)}, u32[]{:S(2)}, u32[]{:S(2)}) collective-permute-start(bf16[136,256]{1,0:T(8,128)(2,1)S(1)} %get-tuple-element.59), channel_id=1, source_target_pairs={{0,160},{32,192},{64,224},{96,0},{128,32},{160,64},{192,96},{224,1... | collective-permute-start | bytes 208904 | tf_op jit(solution)/shard_map/ppermute | solution.py:29
  27.0 11.3 %collective-permute-start.7 = (bf16[4,136,256]{2,1,0:T(8,128)(2,1)S(1)}, bf16[4,136,256]{2,1,0:T(8,128)(2,1)S(1)}, u32[]{:S(2)}, u32[]{:S(2)}) collective-permute-start(bf16[4,136,256]{2,1,0:T(8,128)(2,1)S(1)} %collective-permute-done.5.refs_5_), channel_id=1, source_target_pairs={{0,32},{32,64},{64,96},{96,128},{128,160},{160,192},{192,224},{224... | collective-permute-start | bytes 835592 | tf_op jit(solution)/shard_map/ppermute | solution.py:29
  31.0 3.9 %collective-permute-start.10 = (bf16[136,256]{1,0:T(8,128)(2,1)S(1)}, bf16[136,256]{1,0:T(8,128)(2,1)S(1)}, u32[]{:S(2)}, u32[]{:S(2)}) collective-permute-start(bf16[136,256]{1,0:T(8,128)(2,1)S(1)} %collective-permute-done.9.refs_7_), channel_id=1, source_target_pairs={{0,1},{1,0},{2,3},{3,2},{4,5},{5,4},{6,7},{7,6},{8,9},{9,8},{10,11... | collective-permute-start | bytes 208904 | tf_op jit(solution)/shard_map/ppermute | solution.py:29
  31.6 44.2 %collective-permute-start.15 = (bf16[256,2048]{1,0:T(8,128)(2,1)}, bf16[256,2048]{1,0:T(8,128)(2,1)}, u32[]{:S(2)}, u32[]{:S(2)}) collective-permute-start(bf16[256,2048]{1,0:T(8,128)(2,1)} %refs_0_.1), channel_id=1, source_target_pairs={{0,2},{2,4},{4,6},{6,0},{1,3},{3,5},{5,7},{7,1},{8,10},{10,12},{12... | collective-permute-start | bytes 3145736 | tf_op jit(solution)/shard_map/ppermute | solution.py:29
  33.2 43.2 %collective-permute-start.16 = (bf16[256,2048]{1,0:T(8,128)(2,1)}, bf16[256,2048]{1,0:T(8,128)(2,1)}, u32[]{:S(2)}, u32[]{:S(2)}) collective-permute-start(bf16[256,2048]{1,0:T(8,128)(2,1)} %refs_0_.1), channel_id=1, source_target_pairs={{0,6},{2,0},{4,2},{6,4},{1,7},{3,1},{5,3},{7,5},{8,14},{10,8},{12,... | collective-permute-start | bytes 3145736 | tf_op jit(solution)/shard_map/ppermute | solution.py:29
  35.5 46.9 %collective-permute-start.17 = (bf16[256,2048]{1,0:T(8,128)(2,1)}, bf16[256,2048]{1,0:T(8,128)(2,1)}, u32[]{:S(2)}, u32[]{:S(2)}) collective-permute-start(bf16[256,2048]{1,0:T(8,128)(2,1)} %refs_0_.1), channel_id=1, source_target_pairs={{0,4},{2,6},{4,0},{6,2},{1,5},{3,7},{5,1},{7,3},{8,12},{10,14},{12... | collective-permute-start | bytes 3145736 | tf_op jit(solution)/shard_map/ppermute | solution.py:29
  38.2 1.6 collective-permute-start.6
  38.2 10.3 %collective-permute-start.11 = (bf16[4,136,256]{2,1,0:T(8,128)(2,1)S(1)}, bf16[4,136,256]{2,1,0:T(8,128)(2,1)S(1)}, u32[]{:S(2)}, u32[]{:S(2)}) collective-permute-start(bf16[4,136,256]{2,1,0:T(8,128)(2,1)S(1)} %collective-permute-done.7.refs_5_), channel_id=1, source_target_pairs={{0,32},{32,64},{64,96},{96,128},{128,160},{160,192},{192,224},{224... | collective-permute-start | bytes 835592 | tf_op jit(solution)/shard_map/ppermute | solution.py:29
  39.8 8.7 %collective-permute-start.8 = (bf16[4,136,256]{2,1,0:T(8,128)(2,1)S(1)}, bf16[4,136,256]{2,1,0:T(8,128)(2,1)S(1)}, u32[]{:S(2)}, u32[]{:S(2)}) collective-permute-start(bf16[4,136,256]{2,1,0:T(8,128)(2,1)S(1)} %collective-permute-done.7.refs_5_), channel_id=1, source_target_pairs={{0,1},{1,0},{2,3},{3,2},{4,5},{5,4},{6,7},{7,6},{8,9},{9,8},{10,11... | collective-permute-start | bytes 835592 | tf_op jit(solution)/shard_map/ppermute | solution.py:29
  48.5 9.6 %collective-permute-start.13 = (bf16[4,136,256]{2,1,0:T(8,128)(2,1)S(1)}, bf16[4,136,256]{2,1,0:T(8,128)(2,1)}, u32[]{:S(2)}, u32[]{:S(2)}) collective-permute-start(bf16[4,136,256]{2,1,0:T(8,128)(2,1)S(1)} %collective-permute-done.11.refs_5_), channel_id=1, source_target_pairs={{0,32},{32,64},{64,96},{96,128},{128,160},{160,192},{192,224},{224... | collective-permute-start | bytes 835592 | tf_op jit(solution)/shard_map/ppermute | solution.py:29
  48.5 23.6 %collective-permute-start.12 = (bf16[4,136,256]{2,1,0:T(8,128)(2,1)S(1)}, bf16[4,136,256]{2,1,0:T(8,128)(2,1)}, u32[]{:S(2)}, u32[]{:S(2)}) collective-permute-start(bf16[4,136,256]{2,1,0:T(8,128)(2,1)S(1)} %collective-permute-done.11.refs_5_), channel_id=1, source_target_pairs={{0,1},{1,0},{2,3},{3,2},{4,5},{5,4},{6,7},{7,6},{8,9},{9,8},{10,11... | collective-permute-start | bytes 835592 | tf_op jit(solution)/shard_map/ppermute | solution.py:29
  58.2 15.4 %collective-permute-start.14 = (bf16[4,136,256]{2,1,0:T(8,128)(2,1)}, bf16[4,136,256]{2,1,0:T(8,128)(2,1)}, u32[]{:S(2)}, u32[]{:S(2)}) collective-permute-start(bf16[4,136,256]{2,1,0:T(8,128)(2,1)} %collective-permute-done.13.refs_7_), channel_id=1, source_target_pairs={{0,1},{1,0},{2,3},{3,2},{4,5},{5,4},{6,7},{7,6},{8,9},{9,8},{10,11... | collective-permute-start | bytes 835592 | tf_op jit(solution)/shard_map/ppermute | solution.py:29
  66.0 5.1 %copy-start.20 = (bf16[136,256]{1,0:T(8,128)(2,1)S(1)}, bf16[136,256]{1,0:T(8,128)(2,1)}, u32[]{:S(2)}) copy-start(bf16[136,256]{1,0:T(8,128)(2,1)} %copy-done.19) | copy-start | bytes 208900
  66.0 5.1 %copy-start.22 = (bf16[136,256]{1,0:T(8,128)(2,1)S(1)}, bf16[136,256]{1,0:T(8,128)(2,1)}, u32[]{:S(2)}) copy-start(bf16[136,256]{1,0:T(8,128)(2,1)} %copy-done.21) | copy-start | bytes 208900
  73.5 9.0 %copy-start.7 = (bf16[256,2048]{1,0:T(8,128)(2,1)S(1)}, bf16[256,2048]{1,0:T(8,128)(2,1)}, u32[]{:S(2)}) copy-start(bf16[256,2048]{1,0:T(8,128)(2,1)} %refs_0_.1) | copy-start | bytes 3145732
  73.5 24.2 %copy-start.26 = (s32[5]{0:T(128)S(1)}, s32[5]{0:T(128)}, u32[]{:S(2)}) copy-start(s32[5]{0:T(128)} %stack.19.pos) | copy-start | bytes 64
  73.5 24.2 %copy-start.27 = (f32[2048]{0:T(1024)S(1)}, f32[2048]{0:T(1024)}, u32[]{:S(2)}) copy-start(f32[2048]{0:T(1024)} %param.29) | copy-start | bytes 24580
  75.9 21.8 %collective-permute-start.19 = (bf16[256,2048]{1,0:T(8,128)(2,1)}, bf16[256,2048]{1,0:T(8,128)(2,1)}, u32[]{:S(2)}, u32[]{:S(2)}) collective-permute-start(bf16[256,2048]{1,0:T(8,128)(2,1)} %collective-permute-done.15.refs_1_), channel_id=1, source_target_pairs={{0,1},{1,0},{2,3},{3,2},{4,5},{5,4},{6,7},{7,6},{8,9},{9,8},{10,11... | collective-permute-start | bytes 3145736 | tf_op jit(solution)/shard_map/ppermute | solution.py:29
  76.4 21.3 %collective-permute-start.20 = (bf16[256,2048]{1,0:T(8,128)(2,1)}, bf16[256,2048]{1,0:T(8,128)(2,1)}, u32[]{:S(2)}, u32[]{:S(2)}) collective-permute-start(bf16[256,2048]{1,0:T(8,128)(2,1)} %collective-permute-done.16.refs_2_), channel_id=1, source_target_pairs={{0,1},{1,0},{2,3},{3,2},{4,5},{5,4},{6,7},{7,6},{8,9},{9,8},{10,11... | collective-permute-start | bytes 3145736 | tf_op jit(solution)/shard_map/ppermute | solution.py:29
  82.5 15.2 %collective-permute-start.21 = (bf16[256,2048]{1,0:T(8,128)(2,1)}, bf16[256,2048]{1,0:T(8,128)(2,1)}, u32[]{:S(2)}, u32[]{:S(2)}) collective-permute-start(bf16[256,2048]{1,0:T(8,128)(2,1)} %collective-permute-done.17.refs_3_), channel_id=1, source_target_pairs={{0,1},{1,0},{2,3},{3,2},{4,5},{5,4},{6,7},{7,6},{8,9},{9,8},{10,11... | collective-permute-start | bytes 3145736 | tf_op jit(solution)/shard_map/ppermute | solution.py:29
  82.5 15.2 %collective-permute-start.18 = (bf16[256,2048]{1,0:T(8,128)(2,1)S(1)}, bf16[256,2048]{1,0:T(8,128)(2,1)}, u32[]{:S(2)}, u32[]{:S(2)}) collective-permute-start(bf16[256,2048]{1,0:T(8,128)(2,1)S(1)} %copy-done.7), channel_id=1, source_target_pairs={{0,1},{1,0},{2,3},{3,2},{4,5},{5,4},{6,7},{7,6},{8,9},{9,8},{10,11... | collective-permute-start | bytes 3145736 | tf_op jit(solution)/shard_map/ppermute | solution.py:29
  83.0 14.7 %all-to-all-start = ((bf16[16,32,128]{2,1,0:T(8,128)(2,1)}), bf16[16,32,128]{2,1,0:T(8,128)(2,1)S(1)}, u32[]{:S(2)}, u32[]{:S(2)}) async-start(bf16[16,32,128]{2,1,0:T(8,128)(2,1)} %bitcast.6), calls=%async_computation | async-start | bytes 262144 | tf_op jit(solution)/shard_map/all_to_all | solution.py:480
  97.7 16.7 %copy-start.14 = (bf16[256,256]{1,0:T(8,128)(2,1)S(1)}, bf16[256,256]{1,0:T(8,128)(2,1)}, u32[]{:S(2)}) copy-start(bf16[256,256]{1,0:T(8,128)(2,1)} %copy-done.13) | copy-start | bytes 393220
  97.7 58.6 %copy-start.5 = (bf16[1,2048,512]{2,1,0:T(8,128)(2,1)S(1)}, bf16[1,2048,512]{2,1,0:T(8,128)(2,1)}, u32[]{:S(2)}) copy-start(bf16[1,2048,512]{2,1,0:T(8,128)(2,1)} %up.2) | copy-start | bytes 6291460
  97.7 58.6 %copy-start.6 = (bf16[1,512,2048]{2,1,0:T(8,128)(2,1)S(1)}, bf16[1,512,2048]{2,1,0:T(8,128)(2,1)}, u32[]{:S(2)}) copy-start(bf16[1,512,2048]{2,1,0:T(8,128)(2,1)} %down.2) | copy-start | bytes 6291460
  103.4 52.9 %copy-start.4 = (bf16[1,2048,512]{2,1,0:T(8,128)(2,1)S(1)}, bf16[1,2048,512]{2,1,0:T(8,128)(2,1)}, u32[]{:S(2)}) copy-start(bf16[1,2048,512]{2,1,0:T(8,128)(2,1)} %gate.2) | copy-start | bytes 6291460
  103.4 7.6 %collective-permute-start.22 = (bf16[32,2048]{1,0:T(8,128)(2,1)S(1)}, bf16[32,2048]{1,0:T(8,128)(2,1)S(1)}, u32[]{:S(2)}, u32[]{:S(2)}) collective-permute-start(bf16[32,2048]{1,0:T(8,128)(2,1)S(1)} %get-tuple-element.72.refs_0_), channel_id=1, source_target_pairs={{0,2},{2,4},{4,6},{6,0},{1,3},{3,5},{5,7},{7,1},{8,10},{10,12},{12... | collective-permute-start | bytes 393224 | tf_op jit(solution)/shard_map/ppermute | solution.py:29
  103.8 7.4 %collective-permute-start.23 = (bf16[32,2048]{1,0:T(8,128)(2,1)S(1)}, bf16[32,2048]{1,0:T(8,128)(2,1)S(1)}, u32[]{:S(2)}, u32[]{:S(2)}) collective-permute-start(bf16[32,2048]{1,0:T(8,128)(2,1)S(1)} %get-tuple-element.72.refs_0_), channel_id=1, source_target_pairs={{0,6},{2,0},{4,2},{6,4},{1,7},{3,1},{5,3},{7,5},{8,14},{10,8},{12,... | collective-permute-start | bytes 393224 | tf_op jit(solution)/shard_map/ppermute | solution.py:29
  106.6 6.5 %collective-permute-start.24 = (bf16[32,2048]{1,0:T(8,128)(2,1)S(1)}, bf16[32,2048]{1,0:T(8,128)(2,1)S(1)}, u32[]{:S(2)}, u32[]{:S(2)}) collective-permute-start(bf16[32,2048]{1,0:T(8,128)(2,1)S(1)} %get-tuple-element.72.refs_0_), channel_id=1, source_target_pairs={{0,4},{2,6},{4,0},{6,2},{1,5},{3,7},{5,1},{7,3},{8,12},{10,14},{12... | collective-permute-start | bytes 393224 | tf_op jit(solution)/shard_map/ppermute | solution.py:29
  106.9 6.2 %collective-permute-start.25 = (bf16[32,2048]{1,0:T(8,128)(2,1)S(1)}, bf16[32,2048]{1,0:T(8,128)(2,1)S(1)}, u32[]{:S(2)}, u32[]{:S(2)}) collective-permute-start(bf16[32,2048]{1,0:T(8,128)(2,1)S(1)} %get-tuple-element.72.refs_0_), channel_id=1, source_target_pairs={{0,1},{1,0},{2,3},{3,2},{4,5},{5,4},{6,7},{7,6},{8,9},{9,8},{10,11... | collective-permute-start | bytes 393224 | tf_op jit(solution)/shard_map/ppermute | solution.py:29
  111.0 2.1 %collective-permute-start.26 = (bf16[32,2048]{1,0:T(8,128)(2,1)S(1)}, bf16[32,2048]{1,0:T(8,128)(2,1)S(1)}, u32[]{:S(2)}, u32[]{:S(2)}) collective-permute-start(bf16[32,2048]{1,0:T(8,128)(2,1)S(1)} %collective-permute-done.22.refs_1_), channel_id=1, source_target_pairs={{0,1},{1,0},{2,3},{3,2},{4,5},{5,4},{6,7},{7,6},{8,9},{9,8},{10,11... | collective-permute-start | bytes 393224 | tf_op jit(solution)/shard_map/ppermute | solution.py:29
  111.2 1.9 collective-permute-start.27
  113.1 1.3 collective-permute-start.28
  115.5 40.8 %copy-start.8 = (bf16[256,2048]{1,0:T(8,128)(2,1)}, bf16[256,2048]{1,0:T(8,128)(2,1)S(1)}, u32[]{:S(2)}) copy-start(bf16[256,2048]{1,0:T(8,128)(2,1)S(1)} %get-tuple-element.74.rows) | copy-start | bytes 3145732
  160.2 5.7 %copy-start.33 = (bf16[2048,64]{0,1:T(8,128)(2,1)S(1)}, bf16[2048,64]{0,1:T(8,128)(2,1)}, u32[]{:S(2)}) copy-start(bf16[2048,64]{0,1:T(8,128)(2,1)} %param.35) | copy-start | bytes 786436
  160.2 7.2 %copy-start.10 = (bf16[64,2048]{1,0:T(8,128)(2,1)S(1)}, bf16[64,2048]{1,0:T(8,128)(2,1)}, u32[]{:S(2)}) copy-start(bf16[64,2048]{1,0:T(8,128)(2,1)} %down.3) | copy-start | bytes 786436
  160.2 32.8 %all-to-all-start.2 = ((bf16[32,8,2048]{2,1,0:T(8,128)(2,1)}), bf16[32,8,2048]{2,1,0:T(8,128)(2,1)S(1)}, u32[]{:S(2)}, u32[]{:S(2)}) async-start(bf16[32,8,2048]{2,1,0:T(8,128)(2,1)} %bitcast.14), calls=%async_computation.2 | async-start | bytes 2097152 | tf_op jit(solution)/shard_map/all_to_all | solution.py:516
  168.6 24.3 %copy-start.16 = (bf16[256,256]{1,0:T(8,128)(2,1)S(1)}, bf16[256,256]{1,0:T(8,128)(2,1)}, u32[]{:S(2)}) copy-start(bf16[256,256]{1,0:T(8,128)(2,1)} %copy-done.15) | copy-start | bytes 393220
  193.0 1.6 copy-start.2
  196.2 15.5 %copy-start.12 = (f32[32,2048]{1,0:T(8,128)S(1)}, f32[32,2048]{1,0:T(8,128)}, u32[]{:S(2)}) copy-start(f32[32,2048]{1,0:T(8,128)} %copy-done.11) | copy-start | bytes 786436
  196.2 2.0 collective-permute-start.29
  (18 other events, 14.9 us)
where the time goes:
time: 213 us; the launch traced here: 212 us
  waiting for transfers between devices  72.9 us (34%)
  blocking collectives  54 us (25%)
  starting transfers between devices  39.9 us (19%)
  Pallas kernels  25.4 us (12%)
  local copies, waits for them, and re-layouts  18.9 us (9%)
    all_to_all x1, blocking collectives, layer(): lax.all_to_all(outgoing.reshape(NZ * NX, CAP, D), plane_axes, split_axis=...  40.8 us
    ppermute x26, waiting for transfers between devices, shift(): lax.ppermute(value, axis, [(i, (i + step) % size) for i in range(size)])  40.2 us
    all_to_all x1, waiting for transfers between devices, layer(): lax.all_to_all(result.reshape(NZ * NX, CAP, D), plane_axes, split_axis=0,...  22 us
    ppermute x26, starting transfers between devices, shift(): lax.ppermute(value, axis, [(i, (i + step) % size) for i in range(size)])  20.2 us
    pallas_call x11, Pallas kernels, call(): pl.pallas_call(kernel, out_shape=outs, in_specs=[SMEM] * len(scalars) + [...  19.8 us
    unnamed x72, local copies, waits for them, and re-layouts  18.2 us
    all_to_all x1, blocking collectives, layer(): lax.all_to_all(pair_sum.reshape(NY, 32, D), 'y', split_axis=0, concat_axi...  13.2 us
    all_to_all x1, starting transfers between devices, layer(): lax.all_to_all(heads.reshape(NX * NY, 32, 128), ('x', 'y'), split_axis=0,...  8.29 us
  transfers between devices with their start and end apart: 32, of which 15 were waited for; matrix products, arithmetic and copies ran while one was open for 1% of the time, Pallas kernels for 6%

commit v1 on v0

--- a/solution.py
+++ b/solution.py
@@ -21,7 +21,7 @@
 F32 = jnp.float32
 SMEM = pl.BlockSpec(memory_space=pltpu.SMEM)
 VMEM = pl.BlockSpec(memory_space=pltpu.VMEM)
-VLIM = 28 * 1024 * 1024
+VLIM = 20 * 1024 * 1024
 
 
 def shift(value, axis, step):
@@ -118,7 +118,6 @@
 def unpack_kernel(pos, r0, r1, r2, r3, keys, edge, queries, docs, lam):
     mine = (pos[1] & 1) * 2 + pos[3]
     lane = iota((HALF, 128), 1)
-    unit = (iota((HALF, 128), 0) == lane).astype(BF)
     for turn, ref in enumerate((r0, r1, r2, r3)):
         block = mine ^ turn
         keys[block] = ref[:, 128:384]
@@ -132,18 +131,15 @@
         queries[pl.ds(start, HALF), :] = jnp.where(lane < 64, both, jnp.zeros_like(both))
         queries[pl.ds(start + 512, HALF), :] = jnp.where(lane < 64, jnp.zeros_like(both), both)
         extra = ref[HALF:LINES, 0:128].astype(F32)
-        spread = jnp.broadcast_to(extra[0:1, :], (HALF, 128)).astype(BF)
-        column = lax.dot_general(
-            unit, spread, (((1,), (1,)), ((), ())), preferred_element_type=F32
-        )
-        docs[pl.ds(start, HALF), :] = column
-        docs[pl.ds(start + 512, HALF), :] = column
+        numbers = jnp.broadcast_to(extra[0:1, :], (8, HALF))
+        docs[:, pl.ds(start, HALF)] = numbers
+        docs[:, pl.ds(start + 512, HALF)] = numbers
         if turn == 0:
             total = extra[1:2, :] + extra[2:3, :] + extra[3:4, :]
             lam[...] = jnp.broadcast_to(total, (8, 128))
 
 
-ROWS = 256
+COLS = 256
 
 
 def attend_kernel(kinds, first_call, last_call, pos, *refs):
@@ -158,93 +154,94 @@
         at += 3
     planes = []
     for back, blocks in kinds:
-        count = 2
-        planes.append((back, blocks, refs[at : at + count]))
-        at += count
+        planes.append((back, blocks, refs[at : at + 2]))
+        at += 2
     if last_call:
         out = refs[at]
         tops, sums, acc = refs[at + 1 : at + 4]
+        at += 4
     else:
         tops, sums, acc = refs[at : at + 3]
+        at += 3
+    flipped, key_docs = refs[at : at + 2]
     z, core = pos[0], pos[3]
-    least = jnp.min(query_docs[0:8, :])
-
-    def setup(tile):
-        rows = pl.ds(pl.multiple_of(tile * ROWS, ROWS), ROWS)
-        if first_call:
-            tops[rows, :] = jnp.full((ROWS, 128), NEG_FILL, F32)
-            sums[rows, :] = jnp.zeros((ROWS, 128), F32)
-            acc[rows, :] = jnp.zeros((ROWS, 128), F32)
-        else:
-            for dst, src in zip((tops, sums, acc), state_in):
-                dst[rows, :] = src[rows, :]
-
-    def step(tile, back, blocks, arrays):
-        rows = pl.ds(pl.multiple_of(tile * ROWS, ROWS), ROWS)
+    if first_call:
+        tops[...] = jnp.full((8, 1024), NEG_FILL, F32)
+        sums[...] = jnp.zeros((8, 1024), F32)
+        acc[...] = jnp.zeros((128, 1024), F32)
+    else:
+        for dst, src in zip((tops, sums, acc), state_in):
+            dst[...] = src[...]
+
+    def visit(back, blocks, arrays):
         count = blocks * TOK
+        unit = (iota((HALF, 128), 0) == iota((HALF, 128), 1)).astype(BF)
         parts = [
             ref[:, :] if blocks == 1 else ref[b] for b in range(blocks) for ref in arrays
         ]
-        numbers = jnp.concatenate([p[HALF:LINES, 0:128].astype(F32) for p in parts], axis=1)
-        key_docs = numbers[0:1, :]
-        parts = [p[0:HALF] for p in parts]
-        keys = jnp.concatenate([p[:, 0:128] for p in parts], axis=0)
-        vals = jnp.concatenate([p[:, 128:256] for p in parts], axis=0)
-        raw = lax.dot_general(
-            queries[rows, :], keys, (((1,), (1,)), ((), ())), preferred_element_type=F32
-        )
-        scaled = raw * (0.125 * LOG2E)
-        allowed = key_docs == query_docs[rows, :][:, 0:1]
-        if back == 0:
-            at_key = iota((1, count), 1)
-            lane = at_key & 127
-            key_pos = (
-                (at_key >> 8) * TOK
-                + 64 * (lane >> 5)
-                + 32 * (core ^ ((at_key >> 7) & 1))
-                + (lane & 31)
+        for index, part in enumerate(parts):
+            spread = jnp.broadcast_to(part[HALF : HALF + 1, 0:128].astype(F32), (HALF, 128))
+            key_docs[index * HALF : (index + 1) * HALF, :] = lax.dot_general(
+                unit, spread.astype(BF), (((1,), (1,)), ((), ())), preferred_element_type=F32
             )
-            at_row = (iota((ROWS, 1), 0) + tile * ROWS) & 511
-            row = at_row & 127
-            query_pos = (at_row >> 7) * TOK + 64 * (row >> 5) + 32 * core + (row & 31)
-            allowed = allowed & (key_pos <= query_pos)
-        masked = jnp.where(allowed, scaled, NEG_FILL)
-        old = tops[rows, :][:, 0:1]
-        new = jnp.maximum(old, jnp.max(masked, axis=1, keepdims=True))
-        probs = jnp.exp2(masked - new)
-        fade = jnp.exp2(old - new)
-        tops[rows, :] = jnp.broadcast_to(new, (ROWS, 128))
-        sums[rows, :] = sums[rows, :] * fade + jnp.sum(probs, axis=1, keepdims=True)
-        acc[rows, :] = acc[rows, :] * fade + jnp.dot(
-            probs.astype(BF), vals, preferred_element_type=F32
-        )
-
-    def over_tiles(body):
-        def turn(tile, carry):
-            body(tile)
+            flipped[:, index * HALF : (index + 1) * HALF] = part[0:HALF, 128:256].T
+        keys = jnp.concatenate([p[0:HALF, 0:128] for p in parts], axis=0)
+
+        def tile(step, carry):
+            cols = pl.ds(pl.multiple_of(step * COLS, COLS), COLS)
+            raw = lax.dot_general(
+                keys, queries[cols, :], (((1,), (1,)), ((), ())), preferred_element_type=F32
+            )
+            scaled = raw * (0.125 * LOG2E)
+            numbers = key_docs[0:count, :]
+            numbers = jnp.concatenate([numbers] * (COLS // 128), axis=1)
+            allowed = numbers == query_docs[0:1, cols]
+            if back == 0:
+                at_key = iota((count, 1), 0)
+                line = at_key & 127
+                key_pos = (
+                    (at_key >> 8) * TOK
+                    + 64 * (line >> 5)
+                    + 32 * (core ^ ((at_key >> 7) & 1))
+                    + (line & 31)
+                )
+                at_query = (iota((1, COLS), 1) + step * COLS) & 511
+                line = at_query & 127
+                query_pos = (at_query >> 7) * TOK + 64 * (line >> 5) + 32 * core + (line & 31)
+                allowed = allowed & (key_pos <= query_pos)
+            masked = jnp.where(allowed, scaled, NEG_FILL)
+            old = tops[0:1, cols]
+            new = jnp.maximum(old, jnp.max(masked, axis=0, keepdims=True))
+            probs = jnp.exp2(masked - new)
+            fade = jnp.exp2(old - new)
+            total = sums[0:1, cols] * fade + jnp.sum(probs, axis=0, keepdims=True)
+            tops[:, cols] = jnp.broadcast_to(new, (8, COLS))
+            sums[:, cols] = jnp.broadcast_to(total, (8, COLS))
+            acc[:, cols] = acc[:, cols] * fade + jnp.dot(
+                flipped[:, 0:count], probs.astype(BF), preferred_element_type=F32
+            )
             return carry
 
-        lax.fori_loop(0, 1024 // ROWS, turn, 0)
-
-    over_tiles(setup)
+        lax.fori_loop(0, 1024 // COLS, tile, 0)
+
+    least = jnp.min(query_docs[0:1, 0:128])
     for back, blocks, arrays in planes:
         if back == 0:
-            over_tiles(lambda tile: step(tile, back, blocks, arrays))
+            visit(back, blocks, arrays)
         else:
-
             last = [ref[...] if blocks == 1 else ref[3] for ref in arrays]
             latest = jnp.max(jnp.maximum(*[p[HALF : HALF + 1, 0:128].astype(F32) for p in last]))
 
             @pl.when((z >= back) & (latest >= least))
             def _():
-                over_tiles(lambda tile: step(tile, back, blocks, arrays))
+                visit(back, blocks, arrays)
 
     if last_call:
-        one = acc[0:512, :] / sums[0:512, :]
-        two = acc[512:1024, :] / sums[512:1024, :]
-        head = one - lam[0:1, :] * two
-        scale = lax.rsqrt(jnp.mean(head * head, axis=1, keepdims=True) + 1e-5)
-        out[...] = (head * scale * gain[...] * HEAD_SCALE).astype(BF)
+        one = acc[:, 0:512] / sums[0:1, 0:512]
+        two = acc[:, 512:1024] / sums[0:1, 512:1024]
+        head = one - lam[0:1, 0:1] * two
+        scale = lax.rsqrt(jnp.mean(head * head, axis=0, keepdims=True) + 1e-5)
+        out[...] = ((head * scale).T * gain[...] * HEAD_SCALE).astype(BF)
 
 
 def attend(pos, queries, docs, planes, state=None, finish=None):
@@ -256,37 +253,45 @@
         operands += list(state)
     for _, _, arrays in planes:
         operands += list(arrays)
-    big = jax.ShapeDtypeStruct((1024, 128), F32)
+    row = jax.ShapeDtypeStruct((8, 1024), F32)
+    big = (row, row, jax.ShapeDtypeStruct((128, 1024), F32))
+    work = [pltpu.VMEM((128, 1024), BF), pltpu.VMEM((1024, 128), F32)]
     kernel = partial(attend_kernel, kinds, state is None, finish is not None)
     keys = sum(blocks * TOK for _, blocks in kinds)
     if finish is not None:
         outs = jax.ShapeDtypeStruct((512, 128), BF)
-        scratch = [pltpu.VMEM((1024, 128), F32)] * 3
+        scratch = [pltpu.VMEM(b.shape, F32) for b in big] + work
     else:
-        outs = (big, big, big)
-        scratch = []
+        outs = big
+        scratch = work
     return call(kernel, [pos], operands, outs, scratch, flops=1024 * keys * 512)
 
 
 def project_kernel(pos, attn, resid, gain, *refs):
-    weights, (mixed, normed) = refs[:-2], refs[-2:]
+    weights = refs[:8]
+    mixed, normed, held, left, sums, sems = refs[8:]
     y, core = pos[2], pos[3]
-    total = resid[...].astype(F32)
-    order = []
-    for flip in range(2):
-        for ahead, w in zip((0, 3, 1, 2), weights[4 * flip : 4 * flip + 4]):
-            order.append((w, ahead, flip))
-    for w, ahead, flip in order:
-        src = (y + ahead) & 3
-        head = 2 * (core ^ flip)
-        lhs = jnp.concatenate([attn[head * 4 + src], attn[(head + 1) * 4 + src]], axis=1)
-        total = total + jnp.dot(lhs, w[...], preferred_element_type=F32)
+    for index, w in enumerate(weights):
+        pltpu.make_async_copy(w, held.at[index], sems.at[index]).start()
+    for index in range(8):
+        src = (y + (0, 3, 1, 2)[index % 4]) & 3
+        head = 2 * (core ^ (index // 4))
+        left[index] = jnp.concatenate([attn[head * 4 + src], attn[(head + 1) * 4 + src]], axis=1)
+    sums[...] = resid[...].astype(F32)
+
+    def turn(index, carry):
+        pltpu.make_async_copy(weights[0], held.at[index], sems.at[index]).wait()
+        sums[...] += jnp.dot(left[index], held[index], preferred_element_type=F32)
+        return carry
+
+    lax.fori_loop(0, 8, turn, 0)
+    total = sums[...]
     mixed[...] = total
     scale = lax.rsqrt(jnp.mean(total * total, axis=1, keepdims=True) + 1e-6)
     normed[...] = (total * scale * gain[...]).astype(BF)
 
 
-def route_kernel(pos, routes, weights, pick, high, low):
+def route_kernel(pos, routes, weights, pick, tables):
     core = pos[3]
     group = pos[2] * NC + core
     at = iota((TOK, TOK), 1)
@@ -320,8 +325,8 @@
     pick[...] = jnp.where(chosen, 1.0, 0.0).astype(BF)
     full = jnp.where(chosen, spread, 0.0).T
     upper = full.astype(BF)
-    high[...] = upper
-    low[...] = (full - upper.astype(F32)).astype(BF)
+    tables[:, 0:SLOTS] = upper
+    tables[:, SLOTS : 2 * SLOTS] = (full - upper.astype(F32)).astype(BF)
 
 
 def dispatch_kernel(pos, pick, *refs):
@@ -334,11 +339,18 @@
     outgoing[...] = jnp.dot(pick[...], rows[...], preferred_element_type=F32).astype(BF)
 
 
-def shared_kernel(rows, gate, up, down, out):
-    gated = jnp.dot(rows[...], gate[...], preferred_element_type=F32)
-    lifted = jnp.dot(rows[...], up[...], preferred_element_type=F32)
-    act = (gated / (1.0 + jnp.exp(-gated)) * lifted).astype(BF)
-    out[...] = jnp.dot(act, down[...], preferred_element_type=F32)
+def shared_kernel(rows, gate, up, down, tables, out):
+    out[:, D:] = tables[...]
+
+    def turn(index, carry):
+        part = pl.ds(pl.multiple_of(index * 64, 64), 64)
+        gated = jnp.dot(rows[part, :], gate[...], preferred_element_type=F32)
+        lifted = jnp.dot(rows[part, :], up[...], preferred_element_type=F32)
+        act = (gated / (1.0 + jnp.exp(-gated)) * lifted).astype(BF)
+        out[part, 0:D] = jnp.dot(act, down[...], preferred_element_type=F32).astype(BF)
+        return carry
+
+    lax.fori_loop(0, TOK // 64, turn, 0)
 
 
 def expert_kernel(rows, gate, up, down, out, acc):
@@ -380,14 +392,21 @@
     )(rows, gate, up, down)
 
 
-def combine_kernel(high, low, rows, shared, keep, send):
+def combine_kernel(rows, shared, keep, send):
     total = (
-        jnp.dot(high[...], rows[...], preferred_element_type=F32)
-        + jnp.dot(low[...], rows[...], preferred_element_type=F32)
-        + shared[...]
+        jnp.dot(shared[:, D : D + SLOTS], rows[...], preferred_element_type=F32)
+        + jnp.dot(shared[:, D + SLOTS :], rows[...], preferred_element_type=F32)
+        + shared[:, 0:D].astype(F32)
     ).astype(BF)
     keep[...] = total[:HALF]
     send[...] = total[HALF:]
+
+
+def pair_kernel(pos, keep, got, *outs):
+    y = pos[2]
+    for ahead, out in zip((0, 1, 3, 2), outs):
+        rows = pl.ds(pl.multiple_of(((y + ahead) & 3) * 32, 32), 32)
+        out[...] = (keep[rows, :].astype(F32) + got[rows, :].astype(F32)).astype(BF)
 
 
 def layer(
@@ -444,25 +463,20 @@
             jax.ShapeDtypeStruct((NX, LINES, 256), BF),
             jax.ShapeDtypeStruct((LINES, 256), BF),
             jax.ShapeDtypeStruct((1024, 128), BF),
-            jax.ShapeDtypeStruct((1024, 128), F32),
+            jax.ShapeDtypeStruct((8, 1024), F32),
             jax.ShapeDtypeStruct((8, 128), F32),
         ),
     )
-    table = jax.ShapeDtypeStruct((SLOTS, TOK), BF)
-    pick, weight_high, weight_low = call(
-        route_kernel, [pos], [routes, route_weight], (table, table, table)
-    )
-
-    queries = after(queries, pick, weight_high, weight_low)
     keys1 = shift(keys0, "z", 1)
     back3 = shift(edge, "z", -3)
+    keys6 = shift(keys0, "z", -2)
     state = attend(pos, queries, docs, [(0, 4, [keys0, swap(keys0)])])
     keys2 = shift(keys1, "z", 1)
+    keys4 = shift(keys6, "z", -2)
     state = attend(pos, queries, docs, [(1, 4, [keys1, swap(keys1)])], state)
     keys3 = shift(keys2, "z", 1)
     pair5 = [back3, swap(back3)]
     state = attend(pos, queries, docs, [(2, 4, [keys2, swap(keys2)]), (5, 1, pair5)], state)
-    keys4 = shift(keys3, "z", 1)
     state = attend(pos, queries, docs, [(3, 4, [keys3, swap(keys3)])], state)
     heads = attend(
         pos,
@@ -473,24 +487,41 @@
         finish=(lam, head_gain.reshape(1, 128)),
     )
 
-    held = after(out_weight, packed[0])
-    mine = [out_weight] + [shift(held, "y", k) for k in (1, -1, 2)]
-    full_weight = mine + [swap(after(w, heads)) for w in mine]
+    mine = [out_weight] + [shift(out_weight, "y", k) for k in (1, -1, 2)]
+    full_weight = mine + [
+        swap(after(out_weight, queries)),
+        swap(after(mine[1], heads)),
+        swap(after(mine[2], heads)),
+        swap(after(mine[3], heads)),
+    ]
 
     attn = lax.all_to_all(
         heads.reshape(NX * NY, 32, 128), ("x", "y"), split_axis=0, concat_axis=0, tiled=True
     )
     own_start = (iy * NC + ic) * 32
     resid_own = lax.dynamic_slice_in_dim(resid, own_start, 32, 0)
-    mixed, normed = call(
+    mixed, normed = pl.pallas_call(
         project_kernel,
-        [pos],
-        [attn, resid_own, ffn_gain.reshape(1, D)] + full_weight,
-        (
-            jax.ShapeDtypeStruct((32, D), F32),
-            jax.ShapeDtypeStruct((32, D), BF),
+        out_shape=(jax.ShapeDtypeStruct((32, D), F32), jax.ShapeDtypeStruct((32, D), BF)),
+        in_specs=[SMEM] + [VMEM] * 3 + [any_space] * 8,
+        out_specs=(VMEM, VMEM),
+        scratch_shapes=[
+            pltpu.VMEM((8, 256, D), BF),
+            pltpu.VMEM((8, 32, 256), BF),
+            pltpu.VMEM((32, D), F32),
+            pltpu.SemaphoreType.DMA((8,)),
+        ],
+        compiler_params=pltpu.CompilerParams(vmem_limit_bytes=VLIM),
+        cost_estimate=pl.CostEstimate(
+            flops=2 * 32 * D * D, bytes_accessed=0, transcendentals=0
         ),
-        flops=2 * 32 * D * D,
+        name="project",
+    )(pos, attn, resid_own, ffn_gain.reshape(1, D), *full_weight)
+
+    table = jax.ShapeDtypeStruct((SLOTS, TOK), BF)
+    wide = jax.ShapeDtypeStruct((TOK, 2 * SLOTS), BF)
+    pick, weights = call(
+        route_kernel, [pos], [after(routes, heads), after(route_weight, heads)], (table, wide)
     )
 
     chunks = [normed] + [shift(normed, "y", k) for k in (1, -1, 2)]
@@ -508,8 +539,8 @@
     shared = call(
         shared_kernel,
         [],
-        [rows, shared_gate, shared_up, shared_down],
-        jax.ShapeDtypeStruct((TOK, D), F32),
+        [rows, shared_gate, shared_up, shared_down, weights],
+        jax.ShapeDtypeStruct((TOK, D + 2 * SLOTS), BF),
         flops=2 * TOK * D * 192,
     )
     result = experts(arrived.reshape(SLOTS, D), expert_gate, expert_up, expert_down)
@@ -518,17 +549,15 @@
     ).reshape(SLOTS, D)
     part = jax.ShapeDtypeStruct((HALF, D), BF)
     keep, send = call(
-        combine_kernel,
-        [],
-        [weight_high, weight_low, returned, shared],
-        (part, part),
-        flops=4 * SLOTS * TOK * D,
-    )
-    pair_sum = (keep.astype(F32) + swap(send).astype(F32)).astype(BF)
-    ffn = lax.all_to_all(
-        pair_sum.reshape(NY, 32, D), "y", split_axis=0, concat_axis=0, tiled=True
-    )
-    return (mixed + ffn.astype(F32).sum(axis=0)).astype(BF)
+        combine_kernel, [], [returned, shared], (part, part), flops=4 * SLOTS * TOK * D
+    )
+    chunk = jax.ShapeDtypeStruct((32, D), BF)
+    own, ahead, behind, across = call(pair_kernel, [pos], [keep, swap(send)], (chunk,) * 4)
+    came = [shift(ahead, "y", 1), shift(behind, "y", -1), shift(across, "y", 2)]
+    total = mixed + own.astype(F32)
+    for piece in came:
+        total = total + piece.astype(F32)
+    return total.astype(BF)
 
 
 def solution(mesh):

time: 213 us -> 221 us (1.038)
  waiting for transfers between devices: 72.9 us -> 92.9 us
  blocking collectives: 54 us -> 37.1 us
  starting transfers between devices: 39.9 us -> 50.8 us
  local copies, waits for them, and re-layouts: 18.9 us -> 12.7 us
    ppermute x26 -> x30, waiting for transfers between devices: 40.2 us -> 60.3 us  [shift(): lax.ppermute(value, axis, [(i, (i + step) % size) for i in range(size)])]
    all_to_all x1 -> x0, blocking collectives: 13.2 us -> none  [layer(): lax.all_to_all(pair_sum.reshape(NY, 32, D), 'y', split_axis=0, concat_axi...]
    ppermute x26 -> x30, starting transfers between devices: 20.2 us -> 29.3 us  [shift(): lax.ppermute(value, axis, [(i, (i + step) % size) for i in range(size)])]
    unnamed x72 -> x40, local copies, waits for them, and re-layouts: 18.2 us -> 11.2 us
    pallas_call x11, Pallas kernels: 19.8 us -> 15.4 us  [call(): pl.pallas_call(kernel, out_shape=outs, in_specs=[SMEM] * len(scalars) + [...]
    pallas_call x0 -> x1, Pallas kernels: none -> 3.98 us  [layer(): pl.pallas_call(project_kernel, out_shape=(jax.ShapeDtypeStruct((32, D), F...]
    all_to_all x1, blocking collectives: 40.8 us -> 37.1 us  [layer(): lax.all_to_all(outgoing.reshape(NZ * NX, CAP, D), plane_axes, split_axis=...]
  transfers between devices with their start and end apart: 32 -> 36, of which waited for: 15 -> 17; matrix products, arithmetic and copies ran while one was open for 1% -> 1% of each run, Pallas kernels for 6% -> 5%
where the time goes in v1:
time: 221 us
  waiting for transfers between devices  92.9 us (42%)
  starting transfers between devices  50.8 us (23%)
  blocking collectives  37.1 us (17%)
  Pallas kernels  25.9 us (12%)
  local copies, waits for them, and re-layouts  12.7 us (6%)
    ppermute x30, waiting for transfers between devices, shift(): lax.ppermute(value, axis, [(i, (i + step) % size) for i in range(size)])  60.3 us
    all_to_all x1, blocking collectives, layer(): lax.all_to_all(outgoing.reshape(NZ * NX, CAP, D), plane_axes, split_axis=...  37.1 us
    ppermute x30, starting transfers between devices, shift(): lax.ppermute(value, axis, [(i, (i + step) % size) for i in range(size)])  29.3 us
    all_to_all x1, waiting for transfers between devices, layer(): lax.all_to_all(result.reshape(NZ * NX, CAP, D), plane_axes, split_axis=0,...  21.9 us
    pallas_call x11, Pallas kernels, call(): pl.pallas_call(kernel, out_shape=outs, in_specs=[SMEM] * len(scalars) + [...  15.4 us
    unnamed x40, local copies, waits for them, and re-layouts  11.2 us
    all_to_all x1, starting transfers between devices, layer(): lax.all_to_all(heads.reshape(NX * NY, 32, 128), ('x', 'y'), split_axis=0,...  9.48 us
    all_to_all x1, starting transfers between devices, layer(): lax.all_to_all(result.reshape(NZ * NX, CAP, D), plane_axes, split_axis=0,...  6.36 us
  transfers between devices with their start and end apart: 36, of which 17 were waited for; matrix products, arithmetic and copies ran while one was open for 1% of the time, Pallas kernels for 5%

profile of v1, /device:TPU:2, one launch (start us, length us, event | category | flops | bytes accessed | tf_op | source)
XLA Modules:
  0.0 220.5 jit_solution(12512121548304411978)
XLA Ops:
  0.6 2.8 %pack.1 = (bf16[136,384]{1,0:T(8,128)(2,1)}, bf16[136,384]{1,0:T(8,128)(2,1)}, bf16[136,384]{1,0:T(8,128)(2,1)}, bf16[136,384]{1,0:T(8,128)(2,1)}) custom-call(s32[5]{0:T(128)} %stack.19.pos, f32[2]{0:T(128)} %lam.1, s32[1,256]{1,0:T(1,128)} %bitcast.16, bf16[256,128]{1,0:T(8,128)(2,1)} %q1.1, bf16[256,128]{1,0:T(8,128)(2,1)} %q2.1, bf16[256,128]{1,0:T(8,128)(2,1)} %k1.1, ...), custom_call_target="tpu_custom_call" | custom-call | tf_op jit(solution)/shard_map/pack/pallas_call | solution.py:438
  3.4 1.9 collective-permute-start
  5.3 1.9 collective-permute-start.1
  7.5 1.5 collective-permute-start.3
  9.0 1.8 collective-permute-done.r0
  10.8 2.5 %collective-permute-done.1.r1 = bf16[136,384]{1,0:T(8,128)(2,1)S(1)} collective-permute-done((bf16[136,384]{1,0:T(8,128)(2,1)}, bf16[136,384]{1,0:T(8,128)(2,1)S(1)}, u32[]{:S(2)}, u32[]{:S(2)}) %collective-permute-start.1) | collective-permute-done | bytes 104480 | tf_op jit(solution)/shard_map/ppermute | solution.py:457
  14.6 2.0 collective-permute-start.5
  16.5 2.0 collective-permute-start.4
  18.6 5.4 %collective-permute-start.13 = (bf16[4,136,256]{2,1,0:T(8,128)(2,1)S(1)}, bf16[4,136,256]{2,1,0:T(8,128)(2,1)S(1)}, u32[]{:S(2)}, u32[]{:S(2)}) collective-permute-start(bf16[4,136,256]{2,1,0:T(8,128)(2,1)S(1)} %get-tuple-element.51.refs_2_), channel_id=1, source_target_pairs={{0,192},{32,224},{64,0},{96,32},{128,64},{160,96},{192,128},{224,1... | collective-permute-start | bytes 835592 | tf_op jit(solution)/shard_map/ppermute | solution.py:29
  24.0 3.1 %collective-permute-start.9 = (bf16[136,256]{1,0:T(8,128)(2,1)S(1)}, bf16[136,256]{1,0:T(8,128)(2,1)S(1)}, u32[]{:S(2)}, u32[]{:S(2)}) collective-permute-start(bf16[136,256]{1,0:T(8,128)(2,1)S(1)} %get-tuple-element.58), channel_id=1, source_target_pairs={{0,160},{32,192},{64,224},{96,0},{128,32},{160,64},{192,96},{224,1... | collective-permute-start | bytes 208904 | tf_op jit(solution)/shard_map/ppermute | solution.py:29
  28.0 12.6 %collective-permute-done.9.refs_7_ = bf16[136,256]{1,0:T(8,128)(2,1)S(1)} collective-permute-done((bf16[136,256]{1,0:T(8,128)(2,1)S(1)}, bf16[136,256]{1,0:T(8,128)(2,1)S(1)}, u32[]{:S(2)}, u32[]{:S(2)}) %collective-permute-start.9) | collective-permute-done | bytes 69664 | tf_op jit(solution)/shard_map/ppermute | solution.py:29
  40.6 1.6 collective-permute-start.16
  42.2 2.7 %collective-permute-start.17 = (bf16[256,2048]{1,0:T(8,128)(2,1)}, bf16[256,2048]{1,0:T(8,128)(2,1)}, u32[]{:S(2)}, u32[]{:S(2)}) collective-permute-start(bf16[256,2048]{1,0:T(8,128)(2,1)} %refs_0_.1), channel_id=1, source_target_pairs={{0,6},{2,0},{4,2},{6,4},{1,7},{3,1},{5,3},{7,5},{8,14},{10,8},{12,... | collective-permute-start | bytes 3145736 | tf_op jit(solution)/shard_map/ppermute | solution.py:29
  44.9 1.0 collective-permute-start.18
  45.8 1.0 collective-permute-start.14
  46.8 8.4 %collective-permute-done.7.refs_5_ = bf16[4,136,256]{2,1,0:T(8,128)(2,1)S(1)} collective-permute-done((bf16[4,136,256]{2,1,0:T(8,128)(2,1)S(1)}, bf16[4,136,256]{2,1,0:T(8,128)(2,1)S(1)}, u32[]{:S(2)}, u32[]{:S(2)}) %collective-permute-start.7) | collective-permute-done | bytes 278560 | tf_op jit(solution)/shard_map/ppermute | solution.py:29
  55.3 1.3 collective-permute-start.11
  56.6 6.0 %collective-permute-done.14.refs_7_ = bf16[4,136,256]{2,1,0:T(8,128)(2,1)S(1)} collective-permute-done((bf16[4,136,256]{2,1,0:T(8,128)(2,1)S(1)}, bf16[4,136,256]{2,1,0:T(8,128)(2,1)S(1)}, u32[]{:S(2)}, u32[]{:S(2)}) %collective-permute-start.14) | collective-permute-done | bytes 278560 | tf_op jit(solution)/shard_map/ppermute | solution.py:29
  62.5 1.3 collective-permute-done.11.refs_5_
  64.9 4.4 %shard_map.182 = (f32[8,1024]{1,0:T(8,128)S(1)}, f32[8,1024]{1,0:T(8,128)S(1)}, f32[128,1024]{1,0:T(8,128)S(1)}) custom-call(s32[5]{0:T(128)S(1)} %copy-done.12, bf16[1024,128]{1,0:T(8,128)(2,1)S(1)} %get-tuple-element.48.refs_0_, f32[8,1024]{1,0:T(8,128)S(1)} %get-tuple-element.49.refs_1_, bf16[4,136,256]{2,1,0:T(8,128)(2,1)S(1)} %get-tuple-element.51.refs_2_, ...), custom_call_target="tpu_custom_call" | custom-call | flops 536870912 | tf_op jit(solution)/shard_map/pallas_call | solution.py:41
  71.9 1.5 shard_map.186
  73.7 16.8 %collective-permute-done.17.refs_2_ = bf16[256,2048]{1,0:T(8,128)(2,1)} collective-permute-done((bf16[256,2048]{1,0:T(8,128)(2,1)}, bf16[256,2048]{1,0:T(8,128)(2,1)}, u32[]{:S(2)}, u32[]{:S(2)}) %collective-permute-start.17) | collective-permute-done | bytes 1048608 | tf_op jit(solution)/shard_map/ppermute | solution.py:29
  90.4 1.0 collective-permute-done.18.refs_3_
  91.4 9.5 %all-to-all-start = ((bf16[16,32,128]{2,1,0:T(8,128)(2,1)}), bf16[16,32,128]{2,1,0:T(8,128)(2,1)S(1)}, u32[]{:S(2)}, u32[]{:S(2)}) async-start(bf16[16,32,128]{2,1,0:T(8,128)(2,1)} %bitcast.6), calls=%async_computation | async-start | bytes 262144 | tf_op jit(solution)/shard_map/all_to_all | solution.py:498
  100.9 6.4 %all-to-all-done.attn = bf16[16,32,128]{2,1,0:T(8,128)(2,1)S(1)} async-done(((bf16[16,32,128]{2,1,0:T(8,128)(2,1)}), bf16[16,32,128]{2,1,0:T(8,128)(2,1)S(1)}, u32[]{:S(2)}, u32[]{:S(2)}) %all-to-all-start) | async-done | bytes 131104 | tf_op jit(solution)/shard_map/all_to_all | solution.py:498
  107.3 4.0 %project.1 = (f32[32,2048]{1,0:T(8,128)S(1)}, bf16[32,2048]{1,0:T(8,128)(2,1)S(1)}) custom-call(s32[5]{0:T(128)S(1)} %copy-done.13, bf16[16,32,128]{2,1,0:T(8,128)(2,1)S(1)} %all-to-all-done.attn, bf16[32,2048]{1,0:T(8,128)(2,1)S(1)} %constant_dynamic-slice_fusion.resid, f32[1,2048]{1,0:T(1,128)S(1)} %bitcast.14, bf16[256,2048]{1,0:T(8,128)(2,1)S(1)} %copy-done.5, ...), custom_call_target="tpu_custom_call" | custom-call | flops 268435456 | tf_op jit(solution)/shard_map/project/pallas_call | solution.py:503
  112.5 2.8 %collective-permute-start.24 = (bf16[32,2048]{1,0:T(8,128)(2,1)S(1)}, bf16[32,2048]{1,0:T(8,128)(2,1)S(1)}, u32[]{:S(2)}, u32[]{:S(2)}) collective-permute-start(bf16[32,2048]{1,0:T(8,128)(2,1)S(1)} %get-tuple-element.73.refs_0_), channel_id=1, source_target_pairs={{0,6},{2,0},{4,2},{6,4},{1,7},{3,1},{5,3},{7,5},{8,14},{10,8},{12,... | collective-permute-start | bytes 393224 | tf_op jit(solution)/shard_map/ppermute | solution.py:29
  115.6 4.0 %collective-permute-done.23.refs_1_ = bf16[32,2048]{1,0:T(8,128)(2,1)S(1)} collective-permute-done((bf16[32,2048]{1,0:T(8,128)(2,1)S(1)}, bf16[32,2048]{1,0:T(8,128)(2,1)S(1)}, u32[]{:S(2)}, u32[]{:S(2)}) %collective-permute-start.23) | collective-permute-done | bytes 131104 | tf_op jit(solution)/shard_map/ppermute | solution.py:29
  120.1 1.6 collective-permute-done.25.refs_3_
  122.7 1.1 shard_map.187
  123.9 1.0 shard_map.188
  124.9 1.0 copy-done.6
  125.9 37.1 %all_to_all.15 = bf16[32,8,2048]{2,1,0:T(8,128)(2,1)S(1)} all-to-all(bf16[32,8,2048]{2,1,0:T(8,128)(2,1)S(1)} %bitcast.13), channel_id=1, replica_groups=mesh['z'=8,'x'=4,'y'=4,'c'=2] {'z','x'}, dimensions={0} | all-to-all | bytes 2097152 | tf_op jit(solution)/shard_map/all_to_all | solution.py:536
  163.0 1.6 copy-done.2
  164.6 1.6 copy-done.3
  166.2 1.6 copy-done.4
  167.8 3.8 %expert.1 = bf16[256,2048]{1,0:T(8,128)(2,1)} custom-call(bf16[256,2048]{1,0:T(8,128)(2,1)S(1)} %bitcast.12, bf16[1,2048,512]{2,1,0:T(8,128)(2,1)S(1)} %copy-done.2, bf16[1,2048,512]{2,1,0:T(8,128)(2,1)S(1)} %copy-done.3, bf16[1,512,2048]{2,1,0:T(8,128)(2,1)S(1)} %copy-done.4), custom_call_target="tpu_custom_call" | custom-call | flops 1610612736 | tf_op jit(solution)/shard_map/expert/pallas_call | solution.py:375
  171.5 6.4 %all-to-all-start.2 = ((bf16[32,8,2048]{2,1,0:T(8,128)(2,1)}), bf16[32,8,2048]{2,1,0:T(8,128)(2,1)}, u32[]{:S(2)}, u32[]{:S(2)}) async-start(bf16[32,8,2048]{2,1,0:T(8,128)(2,1)} %bitcast.10), calls=%async_computation.2 | async-start | bytes 2097152 | tf_op jit(solution)/shard_map/all_to_all | solution.py:547
  178.2 1.0 copy.23.up
  179.2 1.0 copy-done.1
  180.3 1.2 copy-done.7
  181.5 2.0 shard_map.189.shared
  183.5 21.9 %all-to-all-done.2 = bf16[32,8,2048]{2,1,0:T(8,128)(2,1)} async-done(((bf16[32,8,2048]{2,1,0:T(8,128)(2,1)}), bf16[32,8,2048]{2,1,0:T(8,128)(2,1)}, u32[]{:S(2)}, u32[]{:S(2)}) %all-to-all-start.2) | async-done | bytes 1048608 | tf_op jit(solution)/shard_map/all_to_all | solution.py:547
  205.4 1.9 shard_map.190
  207.4 1.9 collective-permute-done.30.got
  210.1 3.2 %collective-permute-start.32 = (bf16[32,2048]{1,0:T(8,128)(2,1)S(1)}, bf16[32,2048]{1,0:T(8,128)(2,1)S(1)}, u32[]{:S(2)}, u32[]{:S(2)}) collective-permute-start(bf16[32,2048]{1,0:T(8,128)(2,1)S(1)} %get-tuple-element.81), channel_id=1, source_target_pairs={{0,6},{2,0},{4,2},{6,4},{1,7},{3,1},{5,3},{7,5},{8,14},{10,8},{12,... | collective-permute-start | bytes 393224 | tf_op jit(solution)/shard_map/ppermute | solution.py:29
  213.3 3.5 %collective-permute-done.31 = bf16[32,2048]{1,0:T(8,128)(2,1)S(1)} collective-permute-done((bf16[32,2048]{1,0:T(8,128)(2,1)S(1)}, bf16[32,2048]{1,0:T(8,128)(2,1)S(1)}, u32[]{:S(2)}, u32[]{:S(2)}) %collective-permute-start.31) | collective-permute-done | bytes 131104 | tf_op jit(solution)/shard_map/ppermute | solution.py:29
  216.8 2.1 collective-permute-done.32
  (84 shorter events, 12.7 us)
Async XLA Ops:
  0.0 100.9 %copy-start = (bf16[256,2048]{1,0:T(8,128)(2,1)S(1)}, bf16[256,2048]{1,0:T(8,128)(2,1)}, u32[]{:S(2)}) copy-start(bf16[256,2048]{1,0:T(8,128)(2,1)} %param.19) | copy-start | bytes 3145732
  0.6 68.7 %copy-start.13 = (s32[5]{0:T(128)S(1)}, s32[5]{0:T(128)}, u32[]{:S(2)}) copy-start(s32[5]{0:T(128)} %stack.19.pos) | copy-start | bytes 64
  3.4 7.5 %collective-permute-start = (bf16[136,384]{1,0:T(8,128)(2,1)}, bf16[136,384]{1,0:T(8,128)(2,1)S(1)}, u32[]{:S(2)}, u32[]{:S(2)}) collective-permute-start(bf16[136,384]{1,0:T(8,128)(2,1)} %get-tuple-element.44), channel_id=1, source_target_pairs={{0,0},{1,16},{8,1},{9,17},{16,8},{17,24},{24,9},{25,25},{2,2},{3,1... | collective-permute-start | bytes 313352 | tf_op jit(solution)/shard_map/ppermute | solution.py:457
  5.3 8.0 %collective-permute-start.1 = (bf16[136,384]{1,0:T(8,128)(2,1)}, bf16[136,384]{1,0:T(8,128)(2,1)S(1)}, u32[]{:S(2)}, u32[]{:S(2)}) collective-permute-start(bf16[136,384]{1,0:T(8,128)(2,1)} %get-tuple-element.45), channel_id=1, source_target_pairs={{0,1},{1,17},{8,0},{9,16},{16,9},{17,25},{24,8},{25,24},{2,3},{3,1... | collective-permute-start | bytes 313352 | tf_op jit(solution)/shard_map/ppermute | solution.py:457
  7.2 6.2 %collective-permute-start.2 = (bf16[136,384]{1,0:T(8,128)(2,1)}, bf16[136,384]{1,0:T(8,128)(2,1)S(1)}, u32[]{:S(2)}, u32[]{:S(2)}) collective-permute-start(bf16[136,384]{1,0:T(8,128)(2,1)} %get-tuple-element.46), channel_id=1, source_target_pairs={{0,8},{1,24},{8,9},{9,25},{16,0},{17,16},{24,1},{25,17},{2,10},{3,... | collective-permute-start | bytes 313352 | tf_op jit(solution)/shard_map/ppermute | solution.py:457
  7.5 5.8 %collective-permute-start.3 = (bf16[136,384]{1,0:T(8,128)(2,1)}, bf16[136,384]{1,0:T(8,128)(2,1)S(1)}, u32[]{:S(2)}, u32[]{:S(2)}) collective-permute-start(bf16[136,384]{1,0:T(8,128)(2,1)} %get-tuple-element.47), channel_id=1, source_target_pairs={{0,9},{1,25},{8,8},{9,24},{16,1},{17,17},{24,0},{25,16},{2,11},{3,... | collective-permute-start | bytes 313352 | tf_op jit(solution)/shard_map/ppermute | solution.py:457
  14.6 12.5 %collective-permute-start.5 = (bf16[4,136,256]{2,1,0:T(8,128)(2,1)S(1)}, bf16[4,136,256]{2,1,0:T(8,128)(2,1)S(1)}, u32[]{:S(2)}, u32[]{:S(2)}) collective-permute-start(bf16[4,136,256]{2,1,0:T(8,128)(2,1)S(1)} %get-tuple-element.51.refs_2_), channel_id=1, source_target_pairs={{0,32},{32,64},{64,96},{96,128},{128,160},{160,192},{192,224},{224... | collective-permute-start | bytes 835592 | tf_op jit(solution)/shard_map/ppermute | solution.py:29
  16.5 28.3 %collective-permute-start.4 = (bf16[4,136,256]{2,1,0:T(8,128)(2,1)S(1)}, bf16[4,136,256]{2,1,0:T(8,128)(2,1)S(1)}, u32[]{:S(2)}, u32[]{:S(2)}) collective-permute-start(bf16[4,136,256]{2,1,0:T(8,128)(2,1)S(1)} %get-tuple-element.51.refs_2_), channel_id=1, source_target_pairs={{0,1},{1,0},{2,3},{3,2},{4,5},{5,4},{6,7},{7,6},{8,9},{9,8},{10,11... | collective-permute-start | bytes 835592 | tf_op jit(solution)/shard_map/ppermute | solution.py:29
  18.6 27.3 %collective-permute-start.13 = (bf16[4,136,256]{2,1,0:T(8,128)(2,1)S(1)}, bf16[4,136,256]{2,1,0:T(8,128)(2,1)S(1)}, u32[]{:S(2)}, u32[]{:S(2)}) collective-permute-start(bf16[4,136,256]{2,1,0:T(8,128)(2,1)S(1)} %get-tuple-element.51.refs_2_), channel_id=1, source_target_pairs={{0,192},{32,224},{64,0},{96,32},{128,64},{160,96},{192,128},{224,1... | collective-permute-start | bytes 835592 | tf_op jit(solution)/shard_map/ppermute | solution.py:29
  24.0 16.6 %collective-permute-start.9 = (bf16[136,256]{1,0:T(8,128)(2,1)S(1)}, bf16[136,256]{1,0:T(8,128)(2,1)S(1)}, u32[]{:S(2)}, u32[]{:S(2)}) collective-permute-start(bf16[136,256]{1,0:T(8,128)(2,1)S(1)} %get-tuple-element.58), channel_id=1, source_target_pairs={{0,160},{32,192},{64,224},{96,0},{128,32},{160,64},{192,96},{224,1... | collective-permute-start | bytes 208904 | tf_op jit(solution)/shard_map/ppermute | solution.py:29
  27.1 18.7 %collective-permute-start.6 = (bf16[4,136,256]{2,1,0:T(8,128)(2,1)S(1)}, bf16[4,136,256]{2,1,0:T(8,128)(2,1)S(1)}, u32[]{:S(2)}, u32[]{:S(2)}) collective-permute-start(bf16[4,136,256]{2,1,0:T(8,128)(2,1)S(1)} %collective-permute-done.5.refs_5_), channel_id=1, source_target_pairs={{0,1},{1,0},{2,3},{3,2},{4,5},{5,4},{6,7},{7,6},{8,9},{9,8},{10,11... | collective-permute-start | bytes 835592 | tf_op jit(solution)/shard_map/ppermute | solution.py:29
  40.6 1.6 collective-permute-start.10
  40.6 32.8 %collective-permute-start.16 = (bf16[256,2048]{1,0:T(8,128)(2,1)}, bf16[256,2048]{1,0:T(8,128)(2,1)S(1)}, u32[]{:S(2)}, u32[]{:S(2)}) collective-permute-start(bf16[256,2048]{1,0:T(8,128)(2,1)} %refs_0_.1), channel_id=1, source_target_pairs={{0,2},{2,4},{4,6},{6,0},{1,3},{3,5},{5,7},{7,1},{8,10},{10,12},{12... | collective-permute-start | bytes 3145736 | tf_op jit(solution)/shard_map/ppermute | solution.py:29
  42.2 48.3 %collective-permute-start.17 = (bf16[256,2048]{1,0:T(8,128)(2,1)}, bf16[256,2048]{1,0:T(8,128)(2,1)}, u32[]{:S(2)}, u32[]{:S(2)}) collective-permute-start(bf16[256,2048]{1,0:T(8,128)(2,1)} %refs_0_.1), channel_id=1, source_target_pairs={{0,6},{2,0},{4,2},{6,4},{1,7},{3,1},{5,3},{7,5},{8,14},{10,8},{12,... | collective-permute-start | bytes 3145736 | tf_op jit(solution)/shard_map/ppermute | solution.py:29
  44.9 46.5 %collective-permute-start.18 = (bf16[256,2048]{1,0:T(8,128)(2,1)}, bf16[256,2048]{1,0:T(8,128)(2,1)}, u32[]{:S(2)}, u32[]{:S(2)}) collective-permute-start(bf16[256,2048]{1,0:T(8,128)(2,1)} %refs_0_.1), channel_id=1, source_target_pairs={{0,4},{2,6},{4,0},{6,2},{1,5},{3,7},{5,1},{7,3},{8,12},{10,14},{12... | collective-permute-start | bytes 3145736 | tf_op jit(solution)/shard_map/ppermute | solution.py:29
  45.8 9.4 %collective-permute-start.7 = (bf16[4,136,256]{2,1,0:T(8,128)(2,1)S(1)}, bf16[4,136,256]{2,1,0:T(8,128)(2,1)S(1)}, u32[]{:S(2)}, u32[]{:S(2)}) collective-permute-start(bf16[4,136,256]{2,1,0:T(8,128)(2,1)S(1)} %collective-permute-done.5.refs_5_), channel_id=1, source_target_pairs={{0,32},{32,64},{64,96},{96,128},{128,160},{160,192},{192,224},{224... | collective-permute-start | bytes 835592 | tf_op jit(solution)/shard_map/ppermute | solution.py:29
  45.8 16.7 %collective-permute-start.14 = (bf16[4,136,256]{2,1,0:T(8,128)(2,1)S(1)}, bf16[4,136,256]{2,1,0:T(8,128)(2,1)S(1)}, u32[]{:S(2)}, u32[]{:S(2)}) collective-permute-start(bf16[4,136,256]{2,1,0:T(8,128)(2,1)S(1)} %collective-permute-done.13), channel_id=1, source_target_pairs={{0,192},{32,224},{64,0},{96,32},{128,64},{160,96},{192,128},{224,1... | collective-permute-start | bytes 835592 | tf_op jit(solution)/shard_map/ppermute | solution.py:29
  55.3 8.6 %collective-permute-start.11 = (bf16[4,136,256]{2,1,0:T(8,128)(2,1)S(1)}, bf16[4,136,256]{2,1,0:T(8,128)(2,1)S(1)}, u32[]{:S(2)}, u32[]{:S(2)}) collective-permute-start(bf16[4,136,256]{2,1,0:T(8,128)(2,1)S(1)} %collective-permute-done.7.refs_5_), channel_id=1, source_target_pairs={{0,32},{32,64},{64,96},{96,128},{128,160},{160,192},{192,224},{224... | collective-permute-start | bytes 835592 | tf_op jit(solution)/shard_map/ppermute | solution.py:29
  62.5 1.6 collective-permute-start.8
  63.8 7.0 %collective-permute-start.12 = (bf16[4,136,256]{2,1,0:T(8,128)(2,1)S(1)}, bf16[4,136,256]{2,1,0:T(8,128)(2,1)S(1)}, u32[]{:S(2)}, u32[]{:S(2)}) collective-permute-start(bf16[4,136,256]{2,1,0:T(8,128)(2,1)S(1)} %collective-permute-done.11.refs_5_), channel_id=1, source_target_pairs={{0,1},{1,0},{2,3},{3,2},{4,5},{5,4},{6,7},{7,6},{8,9},{9,8},{10,11... | collective-permute-start | bytes 835592 | tf_op jit(solution)/shard_map/ppermute | solution.py:29
  64.1 7.8 %collective-permute-start.15 = (bf16[4,136,256]{2,1,0:T(8,128)(2,1)S(1)}, bf16[4,136,256]{2,1,0:T(8,128)(2,1)S(1)}, u32[]{:S(2)}, u32[]{:S(2)}) collective-permute-start(bf16[4,136,256]{2,1,0:T(8,128)(2,1)S(1)} %collective-permute-done.14.refs_7_), channel_id=1, source_target_pairs={{0,1},{1,0},{2,3},{3,2},{4,5},{5,4},{6,7},{7,6},{8,9},{9,8},{10,11... | collective-permute-start | bytes 835592 | tf_op jit(solution)/shard_map/ppermute | solution.py:29
  70.0 1.9 copy-start.15
  70.8 30.1 %collective-permute-start.19 = (bf16[256,2048]{1,0:T(8,128)(2,1)S(1)}, bf16[256,2048]{1,0:T(8,128)(2,1)}, u32[]{:S(2)}, u32[]{:S(2)}) collective-permute-start(bf16[256,2048]{1,0:T(8,128)(2,1)S(1)} %copy-done.5), channel_id=1, source_target_pairs={{0,1},{1,0},{2,3},{3,2},{4,5},{5,4},{6,7},{7,6},{8,9},{9,8},{10,11... | collective-permute-start | bytes 3145736 | tf_op jit(solution)/shard_map/ppermute | solution.py:29
  71.2 36.1 %copy-start.14 = (f32[2048]{0:T(1024)S(1)}, f32[2048]{0:T(1024)}, u32[]{:S(2)}) copy-start(f32[2048]{0:T(1024)} %param.29) | copy-start | bytes 24580
  73.4 33.9 %collective-permute-start.20 = (bf16[256,2048]{1,0:T(8,128)(2,1)S(1)}, bf16[256,2048]{1,0:T(8,128)(2,1)}, u32[]{:S(2)}, u32[]{:S(2)}) collective-permute-start(bf16[256,2048]{1,0:T(8,128)(2,1)S(1)} %collective-permute-done.16.refs_1_), channel_id=1, source_target_pairs={{0,1},{1,0},{2,3},{3,2},{4,5},{5,4},{6,7},{7,6},{8,9},{9,8},{10,11... | collective-permute-start | bytes 3145736 | tf_op jit(solution)/shard_map/ppermute | solution.py:29
  90.4 16.9 %collective-permute-start.21 = (bf16[256,2048]{1,0:T(8,128)(2,1)}, bf16[256,2048]{1,0:T(8,128)(2,1)}, u32[]{:S(2)}, u32[]{:S(2)}) collective-permute-start(bf16[256,2048]{1,0:T(8,128)(2,1)} %collective-permute-done.17.refs_2_), channel_id=1, source_target_pairs={{0,1},{1,0},{2,3},{3,2},{4,5},{5,4},{6,7},{7,6},{8,9},{9,8},{10,11... | collective-permute-start | bytes 3145736 | tf_op jit(solution)/shard_map/ppermute | solution.py:29
  91.4 15.9 %collective-permute-start.22 = (bf16[256,2048]{1,0:T(8,128)(2,1)}, bf16[256,2048]{1,0:T(8,128)(2,1)}, u32[]{:S(2)}, u32[]{:S(2)}) collective-permute-start(bf16[256,2048]{1,0:T(8,128)(2,1)} %collective-permute-done.18.refs_3_), channel_id=1, source_target_pairs={{0,1},{1,0},{2,3},{3,2},{4,5},{5,4},{6,7},{7,6},{8,9},{9,8},{10,11... | collective-permute-start | bytes 3145736 | tf_op jit(solution)/shard_map/ppermute | solution.py:29
  91.4 15.9 %all-to-all-start = ((bf16[16,32,128]{2,1,0:T(8,128)(2,1)}), bf16[16,32,128]{2,1,0:T(8,128)(2,1)S(1)}, u32[]{:S(2)}, u32[]{:S(2)}) async-start(bf16[16,32,128]{2,1,0:T(8,128)(2,1)} %bitcast.6), calls=%async_computation | async-start | bytes 262144 | tf_op jit(solution)/shard_map/all_to_all | solution.py:498
  107.3 14.4 %copy-start.18 = (s32[256,4]{0,1:T(4,128)S(1)}, s32[256,4]{0,1:T(4,128)}, u32[]{:S(2)}) copy-start(s32[256,4]{0,1:T(4,128)} %param.30) | copy-start | bytes 12292
  112.0 7.6 %collective-permute-start.23 = (bf16[32,2048]{1,0:T(8,128)(2,1)S(1)}, bf16[32,2048]{1,0:T(8,128)(2,1)S(1)}, u32[]{:S(2)}, u32[]{:S(2)}) collective-permute-start(bf16[32,2048]{1,0:T(8,128)(2,1)S(1)} %get-tuple-element.73.refs_0_), channel_id=1, source_target_pairs={{0,2},{2,4},{4,6},{6,0},{1,3},{3,5},{5,7},{7,1},{8,10},{10,12},{12... | collective-permute-start | bytes 393224 | tf_op jit(solution)/shard_map/ppermute | solution.py:29
  112.5 7.1 %collective-permute-start.24 = (bf16[32,2048]{1,0:T(8,128)(2,1)S(1)}, bf16[32,2048]{1,0:T(8,128)(2,1)S(1)}, u32[]{:S(2)}, u32[]{:S(2)}) collective-permute-start(bf16[32,2048]{1,0:T(8,128)(2,1)S(1)} %get-tuple-element.73.refs_0_), channel_id=1, source_target_pairs={{0,6},{2,0},{4,2},{6,4},{1,7},{3,1},{5,3},{7,5},{8,14},{10,8},{12,... | collective-permute-start | bytes 393224 | tf_op jit(solution)/shard_map/ppermute | solution.py:29
  115.2 6.5 %collective-permute-start.25 = (bf16[32,2048]{1,0:T(8,128)(2,1)S(1)}, bf16[32,2048]{1,0:T(8,128)(2,1)S(1)}, u32[]{:S(2)}, u32[]{:S(2)}) collective-permute-start(bf16[32,2048]{1,0:T(8,128)(2,1)S(1)} %get-tuple-element.73.refs_0_), channel_id=1, source_target_pairs={{0,4},{2,6},{4,0},{6,2},{1,5},{3,7},{5,1},{7,3},{8,12},{10,14},{12... | collective-permute-start | bytes 393224 | tf_op jit(solution)/shard_map/ppermute | solution.py:29
  115.6 8.3 %collective-permute-start.26 = (bf16[32,2048]{1,0:T(8,128)(2,1)S(1)}, bf16[32,2048]{1,0:T(8,128)(2,1)S(1)}, u32[]{:S(2)}, u32[]{:S(2)}) collective-permute-start(bf16[32,2048]{1,0:T(8,128)(2,1)S(1)} %get-tuple-element.73.refs_0_), channel_id=1, source_target_pairs={{0,1},{1,0},{2,3},{3,2},{4,5},{5,4},{6,7},{7,6},{8,9},{9,8},{10,11... | collective-permute-start | bytes 393224 | tf_op jit(solution)/shard_map/ppermute | solution.py:29
  119.6 4.3 %collective-permute-start.27 = (bf16[32,2048]{1,0:T(8,128)(2,1)S(1)}, bf16[32,2048]{1,0:T(8,128)(2,1)S(1)}, u32[]{:S(2)}, u32[]{:S(2)}) collective-permute-start(bf16[32,2048]{1,0:T(8,128)(2,1)S(1)} %collective-permute-done.23.refs_1_), channel_id=1, source_target_pairs={{0,1},{1,0},{2,3},{3,2},{4,5},{5,4},{6,7},{7,6},{8,9},{9,8},{10,11... | collective-permute-start | bytes 393224 | tf_op jit(solution)/shard_map/ppermute | solution.py:29
  119.6 4.3 %collective-permute-start.28 = (bf16[32,2048]{1,0:T(8,128)(2,1)S(1)}, bf16[32,2048]{1,0:T(8,128)(2,1)S(1)}, u32[]{:S(2)}, u32[]{:S(2)}) collective-permute-start(bf16[32,2048]{1,0:T(8,128)(2,1)S(1)} %collective-permute-done.24.refs_2_), channel_id=1, source_target_pairs={{0,1},{1,0},{2,3},{3,2},{4,5},{5,4},{6,7},{7,6},{8,9},{9,8},{10,11... | collective-permute-start | bytes 393224 | tf_op jit(solution)/shard_map/ppermute | solution.py:29
  121.7 2.2 collective-permute-start.29
  163.0 1.6 copy-start.2
  164.6 1.6 copy-start.3
  166.2 1.6 copy-start.4
  171.5 6.4 %copy-start.16 = (bf16[2048,64]{0,1:T(8,128)(2,1)S(1)}, bf16[2048,64]{0,1:T(8,128)(2,1)}, u32[]{:S(2)}) copy-start(bf16[2048,64]{0,1:T(8,128)(2,1)} %param.35) | copy-start | bytes 786436
  171.5 6.7 %copy-start.17 = (bf16[2048,64]{0,1:T(8,128)(2,1)S(1)}, bf16[2048,64]{0,1:T(8,128)(2,1)}, u32[]{:S(2)}) copy-start(bf16[2048,64]{0,1:T(8,128)(2,1)} %param.36) | copy-start | bytes 786436
  171.5 7.7 %copy-start.10 = (bf16[64,2048]{1,0:T(8,128)(2,1)S(1)}, bf16[64,2048]{1,0:T(8,128)(2,1)}, u32[]{:S(2)}) copy-start(bf16[64,2048]{1,0:T(8,128)(2,1)} %down.3) | copy-start | bytes 786436
  171.5 33.8 %all-to-all-start.2 = ((bf16[32,8,2048]{2,1,0:T(8,128)(2,1)}), bf16[32,8,2048]{2,1,0:T(8,128)(2,1)}, u32[]{:S(2)}, u32[]{:S(2)}) async-start(bf16[32,8,2048]{2,1,0:T(8,128)(2,1)} %bitcast.10), calls=%async_computation.2 | async-start | bytes 2097152 | tf_op jit(solution)/shard_map/all_to_all | solution.py:547
  183.5 36.3 %copy-start.9 = (f32[32,2048]{1,0:T(8,128)S(1)}, f32[32,2048]{1,0:T(8,128)}, u32[]{:S(2)}) copy-start(f32[32,2048]{1,0:T(8,128)} %copy-done.8) | copy-start | bytes 786436
  207.3 2.0 collective-permute-start.30
  210.0 6.8 %collective-permute-start.31 = (bf16[32,2048]{1,0:T(8,128)(2,1)S(1)}, bf16[32,2048]{1,0:T(8,128)(2,1)S(1)}, u32[]{:S(2)}, u32[]{:S(2)}) collective-permute-start(bf16[32,2048]{1,0:T(8,128)(2,1)S(1)} %get-tuple-element.80), channel_id=1, source_target_pairs={{0,2},{2,4},{4,6},{6,0},{1,3},{3,5},{5,7},{7,1},{8,10},{10,12},{12... | collective-permute-start | bytes 393224 | tf_op jit(solution)/shard_map/ppermute | solution.py:29
  210.1 8.8 %collective-permute-start.32 = (bf16[32,2048]{1,0:T(8,128)(2,1)S(1)}, bf16[32,2048]{1,0:T(8,128)(2,1)S(1)}, u32[]{:S(2)}, u32[]{:S(2)}) collective-permute-start(bf16[32,2048]{1,0:T(8,128)(2,1)S(1)} %get-tuple-element.81), channel_id=1, source_target_pairs={{0,6},{2,0},{4,2},{6,4},{1,7},{3,1},{5,3},{7,5},{8,14},{10,8},{12,... | collective-permute-start | bytes 393224 | tf_op jit(solution)/shard_map/ppermute | solution.py:29
  213.3 6.5 %collective-permute-start.33 = (bf16[32,2048]{1,0:T(8,128)(2,1)S(1)}, bf16[32,2048]{1,0:T(8,128)(2,1)S(1)}, u32[]{:S(2)}, u32[]{:S(2)}) collective-permute-start(bf16[32,2048]{1,0:T(8,128)(2,1)S(1)} %get-tuple-element.82), channel_id=1, source_target_pairs={{0,4},{2,6},{4,0},{6,2},{1,5},{3,7},{5,1},{7,3},{8,12},{10,14},{12... | collective-permute-start | bytes 393224 | tf_op jit(solution)/shard_map/ppermute | solution.py:29
  (7 other events, 6.6 us)

commit v2 on v1

--- a/solution.py
+++ b/solution.py
@@ -115,17 +115,12 @@
         out[HALF:LINES, 256:384] = extra
 
 
-def unpack_kernel(pos, r0, r1, r2, r3, keys, edge, queries, docs, lam):
+def unpack_kernel(pos, r0, r1, r2, r3, keys, queries, docs, lam):
     mine = (pos[1] & 1) * 2 + pos[3]
     lane = iota((HALF, 128), 1)
     for turn, ref in enumerate((r0, r1, r2, r3)):
         block = mine ^ turn
         keys[block] = ref[:, 128:384]
-
-        @pl.when(block == NX - 1)
-        def _():
-            edge[...] = ref[:, 128:384]
-
         both = ref[0:HALF, 0:128]
         start = pl.multiple_of(block * HALF, HALF)
         queries[pl.ds(start, HALF), :] = jnp.where(lane < 64, both, jnp.zeros_like(both))
@@ -455,29 +450,28 @@
         return pairs
 
     came = [lax.ppermute(packed[t], ("x", "c"), turn_pairs(t)) for t in range(4)]
-    keys0, edge, queries, docs, lam = call(
+    keys0, queries, docs, lam = call(
         unpack_kernel,
         [pos],
         came,
         (
             jax.ShapeDtypeStruct((NX, LINES, 256), BF),
-            jax.ShapeDtypeStruct((LINES, 256), BF),
             jax.ShapeDtypeStruct((1024, 128), BF),
             jax.ShapeDtypeStruct((8, 1024), F32),
             jax.ShapeDtypeStruct((8, 128), F32),
         ),
     )
     keys1 = shift(keys0, "z", 1)
-    back3 = shift(edge, "z", -3)
     keys6 = shift(keys0, "z", -2)
     state = attend(pos, queries, docs, [(0, 4, [keys0, swap(keys0)])])
     keys2 = shift(keys1, "z", 1)
+    back3 = shift(keys6[NX - 1], "z", -1)
     keys4 = shift(keys6, "z", -2)
     state = attend(pos, queries, docs, [(1, 4, [keys1, swap(keys1)])], state)
     keys3 = shift(keys2, "z", 1)
     pair5 = [back3, swap(back3)]
-    state = attend(pos, queries, docs, [(2, 4, [keys2, swap(keys2)]), (5, 1, pair5)], state)
-    state = attend(pos, queries, docs, [(3, 4, [keys3, swap(keys3)])], state)
+    state = attend(pos, queries, docs, [(2, 4, [keys2, swap(keys2)])], state)
+    state = attend(pos, queries, docs, [(3, 4, [keys3, swap(keys3)]), (5, 1, pair5)], state)
     heads = attend(
         pos,
         queries,

time: 221 us -> 212 us (0.959)
  waiting for transfers between devices: 92.9 us -> 86.2 us
    ppermute x30, waiting for transfers between devices: 60.3 us -> 53.6 us  [shift(): lax.ppermute(value, axis, [(i, (i + step) % size) for i in range(size)])]
    all_to_all x1, starting transfers between devices: 9.48 us -> 6.59 us  [layer(): lax.all_to_all(heads.reshape(NX * NY, 32, 128), ('x', 'y'), split_axis=0,...]
  transfers between devices with their start and end apart: 36 -> 36, of which waited for: 17 -> 18; matrix products, arithmetic and copies ran while one was open for 1% -> 1% of each run, Pallas kernels for 5% -> 5%
where the time goes in v2:
time: 212 us
  waiting for transfers between devices  86.2 us (41%)
  starting transfers between devices  49.2 us (23%)
  blocking collectives  36.4 us (17%)
  Pallas kernels  25.9 us (12%)
  local copies, waits for them, and re-layouts  12.8 us (6%)
    ppermute x30, waiting for transfers between devices, shift(): lax.ppermute(value, axis, [(i, (i + step) % size) for i in range(size)])  53.6 us
    all_to_all x1, blocking collectives, layer(): lax.all_to_all(outgoing.reshape(NZ * NX, CAP, D), plane_axes, split_axis=...  36.4 us
    ppermute x30, starting transfers between devices, shift(): lax.ppermute(value, axis, [(i, (i + step) % size) for i in range(size)])  30.5 us
    all_to_all x1, waiting for transfers between devices, layer(): lax.all_to_all(result.reshape(NZ * NX, CAP, D), plane_axes, split_axis=0,...  21.9 us
    pallas_call x11, Pallas kernels, call(): pl.pallas_call(kernel, out_shape=outs, in_specs=[SMEM] * len(scalars) + [...  15.3 us
    unnamed x40, local copies, waits for them, and re-layouts  11.2 us
    all_to_all x1, starting transfers between devices, layer(): lax.all_to_all(heads.reshape(NX * NY, 32, 128), ('x', 'y'), split_axis=0,...  6.59 us
    all_to_all x1, waiting for transfers between devices, layer(): lax.all_to_all(heads.reshape(NX * NY, 32, 128), ('x', 'y'), split_axis=0,...  6.4 us
  transfers between devices with their start and end apart: 36, of which 18 were waited for; matrix products, arithmetic and copies ran while one was open for 1% of the time, Pallas kernels for 5%

profile of v2, /device:TPU:2, one launch (start us, length us, event | category | flops | bytes accessed | tf_op | source)
XLA Modules:
  0.0 211.6 jit_solution(5894510925972772083)
XLA Ops:
  0.6 2.8 %pack.1 = (bf16[136,384]{1,0:T(8,128)(2,1)}, bf16[136,384]{1,0:T(8,128)(2,1)}, bf16[136,384]{1,0:T(8,128)(2,1)}, bf16[136,384]{1,0:T(8,128)(2,1)}) custom-call(s32[5]{0:T(128)} %stack.19.pos, f32[2]{0:T(128)} %lam.1, s32[1,256]{1,0:T(1,128)} %bitcast.18, bf16[256,128]{1,0:T(8,128)(2,1)} %q1.1, bf16[256,128]{1,0:T(8,128)(2,1)} %q2.1, bf16[256,128]{1,0:T(8,128)(2,1)} %k1.1, ...), custom_call_target="tpu_custom_call" | custom-call | tf_op jit(solution)/shard_map/pack/pallas_call | solution.py:433
  3.4 1.9 collective-permute-start
  5.3 1.9 collective-permute-start.1
  7.5 1.5 collective-permute-start.3
  9.0 1.8 collective-permute-done.r0
  10.8 2.5 %collective-permute-done.1.r1 = bf16[136,384]{1,0:T(8,128)(2,1)S(1)} collective-permute-done((bf16[136,384]{1,0:T(8,128)(2,1)}, bf16[136,384]{1,0:T(8,128)(2,1)S(1)}, u32[]{:S(2)}, u32[]{:S(2)}) %collective-permute-start.1) | collective-permute-done | bytes 104480 | tf_op jit(solution)/shard_map/ppermute | solution.py:452
  14.5 2.0 collective-permute-start.5
  16.5 5.4 %collective-permute-start.11 = (bf16[4,136,256]{2,1,0:T(8,128)(2,1)S(1)}, bf16[4,136,256]{2,1,0:T(8,128)(2,1)S(1)}, u32[]{:S(2)}, u32[]{:S(2)}) collective-permute-start(bf16[4,136,256]{2,1,0:T(8,128)(2,1)S(1)} %get-tuple-element.50.refs_2_), channel_id=1, source_target_pairs={{0,192},{32,224},{64,0},{96,32},{128,64},{160,96},{192,128},{224,1... | collective-permute-start | bytes 835592 | tf_op jit(solution)/shard_map/ppermute | solution.py:29
  21.9 1.7 collective-permute-start.4
  23.7 2.7 %collective-permute-done.5.refs_5_ = bf16[4,136,256]{2,1,0:T(8,128)(2,1)S(1)} collective-permute-done((bf16[4,136,256]{2,1,0:T(8,128)(2,1)S(1)}, bf16[4,136,256]{2,1,0:T(8,128)(2,1)S(1)}, u32[]{:S(2)}, u32[]{:S(2)}) %collective-permute-start.5) | collective-permute-done | bytes 278560 | tf_op jit(solution)/shard_map/ppermute | solution.py:29
  26.4 1.4 collective-permute-start.6
  27.8 7.0 %collective-permute-done.11 = bf16[4,136,256]{2,1,0:T(8,128)(2,1)S(1)} collective-permute-done((bf16[4,136,256]{2,1,0:T(8,128)(2,1)S(1)}, bf16[4,136,256]{2,1,0:T(8,128)(2,1)S(1)}, u32[]{:S(2)}, u32[]{:S(2)}) %collective-permute-start.11) | collective-permute-done | bytes 278560 | tf_op jit(solution)/shard_map/ppermute | solution.py:29
  35.2 1.6 collective-permute-start.16
  36.7 1.7 collective-permute-start.17
  38.4 2.0 collective-permute-start.18
  40.4 1.3 collective-permute-done.13.refs_8_
  41.7 1.7 collective-permute-start.7
  43.4 4.6 %collective-permute-start.14 = (bf16[4,136,256]{2,1,0:T(8,128)(2,1)S(1)}, bf16[4,136,256]{2,1,0:T(8,128)(2,1)S(1)}, u32[]{:S(2)}, u32[]{:S(2)}) collective-permute-start(bf16[4,136,256]{2,1,0:T(8,128)(2,1)S(1)} %collective-permute-done.11), channel_id=1, source_target_pairs={{0,192},{32,224},{64,0},{96,32},{128,64},{160,96},{192,128},{224,1... | collective-permute-start | bytes 835592 | tf_op jit(solution)/shard_map/ppermute | solution.py:29
  48.0 5.5 %collective-permute-done.7.refs_5_ = bf16[4,136,256]{2,1,0:T(8,128)(2,1)S(1)} collective-permute-done((bf16[4,136,256]{2,1,0:T(8,128)(2,1)S(1)}, bf16[4,136,256]{2,1,0:T(8,128)(2,1)S(1)}, u32[]{:S(2)}, u32[]{:S(2)}) %collective-permute-start.7) | collective-permute-done | bytes 278560 | tf_op jit(solution)/shard_map/ppermute | solution.py:29
  53.5 6.1 %collective-permute-done.14.refs_7_ = bf16[4,136,256]{2,1,0:T(8,128)(2,1)S(1)} collective-permute-done((bf16[4,136,256]{2,1,0:T(8,128)(2,1)S(1)}, bf16[4,136,256]{2,1,0:T(8,128)(2,1)S(1)}, u32[]{:S(2)}, u32[]{:S(2)}) %collective-permute-start.14) | collective-permute-done | bytes 278560 | tf_op jit(solution)/shard_map/ppermute | solution.py:29
  59.6 3.2 %collective-permute-done.9.refs_5_ = bf16[4,136,256]{2,1,0:T(8,128)(2,1)S(1)} collective-permute-done((bf16[4,136,256]{2,1,0:T(8,128)(2,1)S(1)}, bf16[4,136,256]{2,1,0:T(8,128)(2,1)S(1)}, u32[]{:S(2)}, u32[]{:S(2)}) %collective-permute-start.9) | collective-permute-done | bytes 278560 | tf_op jit(solution)/shard_map/ppermute | solution.py:29
  63.9 4.4 %shard_map.182 = (f32[8,1024]{1,0:T(8,128)S(1)}, f32[8,1024]{1,0:T(8,128)S(1)}, f32[128,1024]{1,0:T(8,128)S(1)}) custom-call(s32[5]{0:T(128)S(1)} %copy-done.12, bf16[1024,128]{1,0:T(8,128)(2,1)S(1)} %get-tuple-element.47.refs_0_, f32[8,1024]{1,0:T(8,128)S(1)} %get-tuple-element.48.refs_1_, bf16[4,136,256]{2,1,0:T(8,128)(2,1)S(1)} %get-tuple-element.50.refs_2_, ...), custom_call_target="tpu_custom_call" | custom-call | flops 536870912 | tf_op jit(solution)/shard_map/pallas_call | solution.py:41
  70.6 1.5 shard_map.186
  72.7 13.2 %collective-permute-done.18.refs_3_ = bf16[256,2048]{1,0:T(8,128)(2,1)} collective-permute-done((bf16[256,2048]{1,0:T(8,128)(2,1)}, bf16[256,2048]{1,0:T(8,128)(2,1)}, u32[]{:S(2)}, u32[]{:S(2)}) %collective-permute-start.18) | collective-permute-done | bytes 1048608 | tf_op jit(solution)/shard_map/ppermute | solution.py:29
  85.9 6.6 %all-to-all-start = ((bf16[16,32,128]{2,1,0:T(8,128)(2,1)}), bf16[16,32,128]{2,1,0:T(8,128)(2,1)S(1)}, u32[]{:S(2)}, u32[]{:S(2)}) async-start(bf16[16,32,128]{2,1,0:T(8,128)(2,1)} %bitcast.7), calls=%async_computation | async-start | bytes 262144 | tf_op jit(solution)/shard_map/all_to_all | solution.py:492
  92.5 6.4 %all-to-all-done.attn = bf16[16,32,128]{2,1,0:T(8,128)(2,1)S(1)} async-done(((bf16[16,32,128]{2,1,0:T(8,128)(2,1)}), bf16[16,32,128]{2,1,0:T(8,128)(2,1)S(1)}, u32[]{:S(2)}, u32[]{:S(2)}) %all-to-all-start) | async-done | bytes 131104 | tf_op jit(solution)/shard_map/all_to_all | solution.py:492
  99.0 4.0 %project.1 = (f32[32,2048]{1,0:T(8,128)S(1)}, bf16[32,2048]{1,0:T(8,128)(2,1)S(1)}) custom-call(s32[5]{0:T(128)S(1)} %copy-done.13, bf16[16,32,128]{2,1,0:T(8,128)(2,1)S(1)} %all-to-all-done.attn, bf16[32,2048]{1,0:T(8,128)(2,1)S(1)} %constant_dynamic-slice_fusion.resid, f32[1,2048]{1,0:T(1,128)S(1)} %bitcast.16, bf16[256,2048]{1,0:T(8,128)(2,1)S(1)} %copy-done.5, ...), custom_call_target="tpu_custom_call" | custom-call | flops 268435456 | tf_op jit(solution)/shard_map/project/pallas_call | solution.py:497
  104.1 2.8 %collective-permute-start.24 = (bf16[32,2048]{1,0:T(8,128)(2,1)S(1)}, bf16[32,2048]{1,0:T(8,128)(2,1)S(1)}, u32[]{:S(2)}, u32[]{:S(2)}) collective-permute-start(bf16[32,2048]{1,0:T(8,128)(2,1)S(1)} %get-tuple-element.71.refs_0_), channel_id=1, source_target_pairs={{0,6},{2,0},{4,2},{6,4},{1,7},{3,1},{5,3},{7,5},{8,14},{10,8},{12,... | collective-permute-start | bytes 393224 | tf_op jit(solution)/shard_map/ppermute | solution.py:29
  107.2 2.6 %collective-permute-done.23.refs_1_ = bf16[32,2048]{1,0:T(8,128)(2,1)S(1)} collective-permute-done((bf16[32,2048]{1,0:T(8,128)(2,1)S(1)}, bf16[32,2048]{1,0:T(8,128)(2,1)S(1)}, u32[]{:S(2)}, u32[]{:S(2)}) %collective-permute-start.23) | collective-permute-done | bytes 131104 | tf_op jit(solution)/shard_map/ppermute | solution.py:29
  109.8 1.9 collective-permute-done.24.refs_2_
  111.8 1.6 collective-permute-done.25.refs_3_
  114.3 1.1 shard_map.187
  115.5 1.0 shard_map.188
  117.6 36.4 %all_to_all.15 = bf16[32,8,2048]{2,1,0:T(8,128)(2,1)S(1)} all-to-all(bf16[32,8,2048]{2,1,0:T(8,128)(2,1)S(1)} %bitcast.15), channel_id=1, replica_groups=mesh['z'=8,'x'=4,'y'=4,'c'=2] {'z','x'}, dimensions={0} | all-to-all | bytes 2097152 | tf_op jit(solution)/shard_map/all_to_all | solution.py:530
  154.0 1.6 copy-done.2
  155.6 1.6 copy-done.3
  157.2 1.6 copy-done.4
  158.8 3.8 %expert.1 = bf16[256,2048]{1,0:T(8,128)(2,1)} custom-call(bf16[256,2048]{1,0:T(8,128)(2,1)S(1)} %bitcast.14, bf16[1,2048,512]{2,1,0:T(8,128)(2,1)S(1)} %copy-done.2, bf16[1,2048,512]{2,1,0:T(8,128)(2,1)S(1)} %copy-done.3, bf16[1,512,2048]{2,1,0:T(8,128)(2,1)S(1)} %copy-done.4), custom_call_target="tpu_custom_call" | custom-call | flops 1610612736 | tf_op jit(solution)/shard_map/expert/pallas_call | solution.py:370
  162.6 6.4 %all-to-all-start.2 = ((bf16[32,8,2048]{2,1,0:T(8,128)(2,1)}), bf16[32,8,2048]{2,1,0:T(8,128)(2,1)}, u32[]{:S(2)}, u32[]{:S(2)}) async-start(bf16[32,8,2048]{2,1,0:T(8,128)(2,1)} %bitcast.11), calls=%async_computation.2 | async-start | bytes 2097152 | tf_op jit(solution)/shard_map/all_to_all | solution.py:541
  170.3 1.0 copy-done.1
  171.3 1.2 copy-done.7
  172.5 1.9 shard_map.189.shared
  174.5 21.9 %all-to-all-done.2 = bf16[32,8,2048]{2,1,0:T(8,128)(2,1)} async-done(((bf16[32,8,2048]{2,1,0:T(8,128)(2,1)}), bf16[32,8,2048]{2,1,0:T(8,128)(2,1)}, u32[]{:S(2)}, u32[]{:S(2)}) %all-to-all-start.2) | async-done | bytes 1048608 | tf_op jit(solution)/shard_map/all_to_all | solution.py:541
  196.4 1.9 shard_map.190
  198.4 1.9 collective-permute-done.30.got
  201.1 3.2 %collective-permute-start.32 = (bf16[32,2048]{1,0:T(8,128)(2,1)S(1)}, bf16[32,2048]{1,0:T(8,128)(2,1)S(1)}, u32[]{:S(2)}, u32[]{:S(2)}) collective-permute-start(bf16[32,2048]{1,0:T(8,128)(2,1)S(1)} %get-tuple-element.79), channel_id=1, source_target_pairs={{0,6},{2,0},{4,2},{6,4},{1,7},{3,1},{5,3},{7,5},{8,14},{10,8},{12,... | collective-permute-start | bytes 393224 | tf_op jit(solution)/shard_map/ppermute | solution.py:29
  204.3 3.5 %collective-permute-done.31 = bf16[32,2048]{1,0:T(8,128)(2,1)S(1)} collective-permute-done((bf16[32,2048]{1,0:T(8,128)(2,1)S(1)}, bf16[32,2048]{1,0:T(8,128)(2,1)S(1)}, u32[]{:S(2)}, u32[]{:S(2)}) %collective-permute-start.31) | collective-permute-done | bytes 131104 | tf_op jit(solution)/shard_map/ppermute | solution.py:29
  207.8 2.1 collective-permute-done.32
  (85 shorter events, 13.7 us)
Async XLA Ops:
  0.0 92.5 %copy-start = (bf16[256,2048]{1,0:T(8,128)(2,1)S(1)}, bf16[256,2048]{1,0:T(8,128)(2,1)}, u32[]{:S(2)}) copy-start(bf16[256,2048]{1,0:T(8,128)(2,1)} %param.19) | copy-start | bytes 3145732
  0.6 67.7 %copy-start.13 = (s32[5]{0:T(128)S(1)}, s32[5]{0:T(128)}, u32[]{:S(2)}) copy-start(s32[5]{0:T(128)} %stack.19.pos) | copy-start | bytes 64
  3.4 7.5 %collective-permute-start = (bf16[136,384]{1,0:T(8,128)(2,1)}, bf16[136,384]{1,0:T(8,128)(2,1)S(1)}, u32[]{:S(2)}, u32[]{:S(2)}) collective-permute-start(bf16[136,384]{1,0:T(8,128)(2,1)} %get-tuple-element.43), channel_id=1, source_target_pairs={{0,0},{1,16},{8,1},{9,17},{16,8},{17,24},{24,9},{25,25},{2,2},{3,1... | collective-permute-start | bytes 313352 | tf_op jit(solution)/shard_map/ppermute | solution.py:452
  5.3 8.0 %collective-permute-start.1 = (bf16[136,384]{1,0:T(8,128)(2,1)}, bf16[136,384]{1,0:T(8,128)(2,1)S(1)}, u32[]{:S(2)}, u32[]{:S(2)}) collective-permute-start(bf16[136,384]{1,0:T(8,128)(2,1)} %get-tuple-element.44), channel_id=1, source_target_pairs={{0,1},{1,17},{8,0},{9,16},{16,9},{17,25},{24,8},{25,24},{2,3},{3,1... | collective-permute-start | bytes 313352 | tf_op jit(solution)/shard_map/ppermute | solution.py:452
  7.2 6.2 %collective-permute-start.2 = (bf16[136,384]{1,0:T(8,128)(2,1)}, bf16[136,384]{1,0:T(8,128)(2,1)S(1)}, u32[]{:S(2)}, u32[]{:S(2)}) collective-permute-start(bf16[136,384]{1,0:T(8,128)(2,1)} %get-tuple-element.45), channel_id=1, source_target_pairs={{0,8},{1,24},{8,9},{9,25},{16,0},{17,16},{24,1},{25,17},{2,10},{3,... | collective-permute-start | bytes 313352 | tf_op jit(solution)/shard_map/ppermute | solution.py:452
  7.5 5.8 %collective-permute-start.3 = (bf16[136,384]{1,0:T(8,128)(2,1)}, bf16[136,384]{1,0:T(8,128)(2,1)S(1)}, u32[]{:S(2)}, u32[]{:S(2)}) collective-permute-start(bf16[136,384]{1,0:T(8,128)(2,1)} %get-tuple-element.46), channel_id=1, source_target_pairs={{0,9},{1,25},{8,8},{9,24},{16,1},{17,17},{24,0},{25,16},{2,11},{3,... | collective-permute-start | bytes 313352 | tf_op jit(solution)/shard_map/ppermute | solution.py:452
  14.5 11.8 %collective-permute-start.5 = (bf16[4,136,256]{2,1,0:T(8,128)(2,1)S(1)}, bf16[4,136,256]{2,1,0:T(8,128)(2,1)S(1)}, u32[]{:S(2)}, u32[]{:S(2)}) collective-permute-start(bf16[4,136,256]{2,1,0:T(8,128)(2,1)S(1)} %get-tuple-element.50.refs_2_), channel_id=1, source_target_pairs={{0,32},{32,64},{64,96},{96,128},{128,160},{160,192},{192,224},{224... | collective-permute-start | bytes 835592 | tf_op jit(solution)/shard_map/ppermute | solution.py:29
  16.5 18.3 %collective-permute-start.11 = (bf16[4,136,256]{2,1,0:T(8,128)(2,1)S(1)}, bf16[4,136,256]{2,1,0:T(8,128)(2,1)S(1)}, u32[]{:S(2)}, u32[]{:S(2)}) collective-permute-start(bf16[4,136,256]{2,1,0:T(8,128)(2,1)S(1)} %get-tuple-element.50.refs_2_), channel_id=1, source_target_pairs={{0,192},{32,224},{64,0},{96,32},{128,64},{160,96},{192,128},{224,1... | collective-permute-start | bytes 835592 | tf_op jit(solution)/shard_map/ppermute | solution.py:29
  21.9 16.5 %collective-permute-start.4 = (bf16[4,136,256]{2,1,0:T(8,128)(2,1)S(1)}, bf16[4,136,256]{2,1,0:T(8,128)(2,1)S(1)}, u32[]{:S(2)}, u32[]{:S(2)}) collective-permute-start(bf16[4,136,256]{2,1,0:T(8,128)(2,1)S(1)} %get-tuple-element.50.refs_2_), channel_id=1, source_target_pairs={{0,1},{1,0},{2,3},{3,2},{4,5},{5,4},{6,7},{7,6},{8,9},{9,8},{10,11... | collective-permute-start | bytes 835592 | tf_op jit(solution)/shard_map/ppermute | solution.py:29
  26.4 17.0 %collective-permute-start.6 = (bf16[4,136,256]{2,1,0:T(8,128)(2,1)S(1)}, bf16[4,136,256]{2,1,0:T(8,128)(2,1)S(1)}, u32[]{:S(2)}, u32[]{:S(2)}) collective-permute-start(bf16[4,136,256]{2,1,0:T(8,128)(2,1)S(1)} %collective-permute-done.5.refs_5_), channel_id=1, source_target_pairs={{0,1},{1,0},{2,3},{3,2},{4,5},{5,4},{6,7},{7,6},{8,9},{9,8},{10,11... | collective-permute-start | bytes 835592 | tf_op jit(solution)/shard_map/ppermute | solution.py:29
  34.8 5.6 %collective-permute-start.12 = (bf16[136,256]{1,0:T(8,128)(2,1)S(1)}, bf16[136,256]{1,0:T(8,128)(2,1)S(1)}, u32[]{:S(2)}, u32[]{:S(2)}) collective-permute-start(bf16[136,256]{1,0:T(8,128)(2,1)S(1)} %slice_bitcast_fusion), channel_id=1, source_target_pairs={{0,224},{32,0},{64,32},{96,64},{128,96},{160,128},{192,160},{224,1... | collective-permute-start | bytes 208904 | tf_op jit(solution)/shard_map/ppermute | solution.py:29
  35.2 37.0 %collective-permute-start.16 = (bf16[256,2048]{1,0:T(8,128)(2,1)}, bf16[256,2048]{1,0:T(8,128)(2,1)S(1)}, u32[]{:S(2)}, u32[]{:S(2)}) collective-permute-start(bf16[256,2048]{1,0:T(8,128)(2,1)} %refs_0_.1), channel_id=1, source_target_pairs={{0,2},{2,4},{4,6},{6,0},{1,3},{3,5},{5,7},{7,1},{8,10},{10,12},{12... | collective-permute-start | bytes 3145736 | tf_op jit(solution)/shard_map/ppermute | solution.py:29
  36.7 35.9 %collective-permute-start.17 = (bf16[256,2048]{1,0:T(8,128)(2,1)}, bf16[256,2048]{1,0:T(8,128)(2,1)}, u32[]{:S(2)}, u32[]{:S(2)}) collective-permute-start(bf16[256,2048]{1,0:T(8,128)(2,1)} %refs_0_.1), channel_id=1, source_target_pairs={{0,6},{2,0},{4,2},{6,4},{1,7},{3,1},{5,3},{7,5},{8,14},{10,8},{12,... | collective-permute-start | bytes 3145736 | tf_op jit(solution)/shard_map/ppermute | solution.py:29
  38.4 47.5 %collective-permute-start.18 = (bf16[256,2048]{1,0:T(8,128)(2,1)}, bf16[256,2048]{1,0:T(8,128)(2,1)}, u32[]{:S(2)}, u32[]{:S(2)}) collective-permute-start(bf16[256,2048]{1,0:T(8,128)(2,1)} %refs_0_.1), channel_id=1, source_target_pairs={{0,4},{2,6},{4,0},{6,2},{1,5},{3,7},{5,1},{7,3},{8,12},{10,14},{12... | collective-permute-start | bytes 3145736 | tf_op jit(solution)/shard_map/ppermute | solution.py:29
  40.4 1.3 collective-permute-start.13
  41.7 11.8 %collective-permute-start.7 = (bf16[4,136,256]{2,1,0:T(8,128)(2,1)S(1)}, bf16[4,136,256]{2,1,0:T(8,128)(2,1)S(1)}, u32[]{:S(2)}, u32[]{:S(2)}) collective-permute-start(bf16[4,136,256]{2,1,0:T(8,128)(2,1)S(1)} %collective-permute-done.5.refs_5_), channel_id=1, source_target_pairs={{0,32},{32,64},{64,96},{96,128},{128,160},{160,192},{192,224},{224... | collective-permute-start | bytes 835592 | tf_op jit(solution)/shard_map/ppermute | solution.py:29
  43.4 16.2 %collective-permute-start.14 = (bf16[4,136,256]{2,1,0:T(8,128)(2,1)S(1)}, bf16[4,136,256]{2,1,0:T(8,128)(2,1)S(1)}, u32[]{:S(2)}, u32[]{:S(2)}) collective-permute-start(bf16[4,136,256]{2,1,0:T(8,128)(2,1)S(1)} %collective-permute-done.11), channel_id=1, source_target_pairs={{0,192},{32,224},{64,0},{96,32},{128,64},{160,96},{192,128},{224,1... | collective-permute-start | bytes 835592 | tf_op jit(solution)/shard_map/ppermute | solution.py:29
  53.5 9.4 %collective-permute-start.9 = (bf16[4,136,256]{2,1,0:T(8,128)(2,1)S(1)}, bf16[4,136,256]{2,1,0:T(8,128)(2,1)S(1)}, u32[]{:S(2)}, u32[]{:S(2)}) collective-permute-start(bf16[4,136,256]{2,1,0:T(8,128)(2,1)S(1)} %collective-permute-done.7.refs_5_), channel_id=1, source_target_pairs={{0,32},{32,64},{64,96},{96,128},{128,160},{160,192},{192,224},{224... | collective-permute-start | bytes 835592 | tf_op jit(solution)/shard_map/ppermute | solution.py:29
  59.6 3.2 %collective-permute-start.8 = (bf16[4,136,256]{2,1,0:T(8,128)(2,1)S(1)}, bf16[4,136,256]{2,1,0:T(8,128)(2,1)S(1)}, u32[]{:S(2)}, u32[]{:S(2)}) collective-permute-start(bf16[4,136,256]{2,1,0:T(8,128)(2,1)S(1)} %collective-permute-done.7.refs_5_), channel_id=1, source_target_pairs={{0,1},{1,0},{2,3},{3,2},{4,5},{5,4},{6,7},{7,6},{8,9},{9,8},{10,11... | collective-permute-start | bytes 835592 | tf_op jit(solution)/shard_map/ppermute | solution.py:29
  62.8 6.8 %collective-permute-start.10 = (bf16[4,136,256]{2,1,0:T(8,128)(2,1)S(1)}, bf16[4,136,256]{2,1,0:T(8,128)(2,1)S(1)}, u32[]{:S(2)}, u32[]{:S(2)}) collective-permute-start(bf16[4,136,256]{2,1,0:T(8,128)(2,1)S(1)} %collective-permute-done.9.refs_5_), channel_id=1, source_target_pairs={{0,1},{1,0},{2,3},{3,2},{4,5},{5,4},{6,7},{7,6},{8,9},{9,8},{10,11... | collective-permute-start | bytes 835592 | tf_op jit(solution)/shard_map/ppermute | solution.py:29
  62.8 7.8 %collective-permute-start.15 = (bf16[4,136,256]{2,1,0:T(8,128)(2,1)S(1)}, bf16[4,136,256]{2,1,0:T(8,128)(2,1)S(1)}, u32[]{:S(2)}, u32[]{:S(2)}) collective-permute-start(bf16[4,136,256]{2,1,0:T(8,128)(2,1)S(1)} %collective-permute-done.14.refs_7_), channel_id=1, source_target_pairs={{0,1},{1,0},{2,3},{3,2},{4,5},{5,4},{6,7},{7,6},{8,9},{9,8},{10,11... | collective-permute-start | bytes 835592 | tf_op jit(solution)/shard_map/ppermute | solution.py:29
  69.0 1.6 copy-start.15
  69.7 22.8 %collective-permute-start.19 = (bf16[256,2048]{1,0:T(8,128)(2,1)S(1)}, bf16[256,2048]{1,0:T(8,128)(2,1)}, u32[]{:S(2)}, u32[]{:S(2)}) collective-permute-start(bf16[256,2048]{1,0:T(8,128)(2,1)S(1)} %copy-done.5), channel_id=1, source_target_pairs={{0,1},{1,0},{2,3},{3,2},{4,5},{5,4},{6,7},{7,6},{8,9},{9,8},{10,11... | collective-permute-start | bytes 3145736 | tf_op jit(solution)/shard_map/ppermute | solution.py:29
  69.8 29.2 %copy-start.14 = (f32[2048]{0:T(1024)S(1)}, f32[2048]{0:T(1024)}, u32[]{:S(2)}) copy-start(f32[2048]{0:T(1024)} %param.29) | copy-start | bytes 24580
  72.1 26.8 %collective-permute-start.20 = (bf16[256,2048]{1,0:T(8,128)(2,1)S(1)}, bf16[256,2048]{1,0:T(8,128)(2,1)}, u32[]{:S(2)}, u32[]{:S(2)}) collective-permute-start(bf16[256,2048]{1,0:T(8,128)(2,1)S(1)} %collective-permute-done.16.refs_1_), channel_id=1, source_target_pairs={{0,1},{1,0},{2,3},{3,2},{4,5},{5,4},{6,7},{7,6},{8,9},{9,8},{10,11... | collective-permute-start | bytes 3145736 | tf_op jit(solution)/shard_map/ppermute | solution.py:29
  72.6 26.3 %collective-permute-start.21 = (bf16[256,2048]{1,0:T(8,128)(2,1)}, bf16[256,2048]{1,0:T(8,128)(2,1)}, u32[]{:S(2)}, u32[]{:S(2)}) collective-permute-start(bf16[256,2048]{1,0:T(8,128)(2,1)} %collective-permute-done.17.refs_2_), channel_id=1, source_target_pairs={{0,1},{1,0},{2,3},{3,2},{4,5},{5,4},{6,7},{7,6},{8,9},{9,8},{10,11... | collective-permute-start | bytes 3145736 | tf_op jit(solution)/shard_map/ppermute | solution.py:29
  85.9 13.0 %collective-permute-start.22 = (bf16[256,2048]{1,0:T(8,128)(2,1)}, bf16[256,2048]{1,0:T(8,128)(2,1)}, u32[]{:S(2)}, u32[]{:S(2)}) collective-permute-start(bf16[256,2048]{1,0:T(8,128)(2,1)} %collective-permute-done.18.refs_3_), channel_id=1, source_target_pairs={{0,1},{1,0},{2,3},{3,2},{4,5},{5,4},{6,7},{7,6},{8,9},{9,8},{10,11... | collective-permute-start | bytes 3145736 | tf_op jit(solution)/shard_map/ppermute | solution.py:29
  85.9 13.0 %all-to-all-start = ((bf16[16,32,128]{2,1,0:T(8,128)(2,1)}), bf16[16,32,128]{2,1,0:T(8,128)(2,1)S(1)}, u32[]{:S(2)}, u32[]{:S(2)}) async-start(bf16[16,32,128]{2,1,0:T(8,128)(2,1)} %bitcast.7), calls=%async_computation | async-start | bytes 262144 | tf_op jit(solution)/shard_map/all_to_all | solution.py:492
  98.9 14.4 %copy-start.18 = (s32[256,4]{0,1:T(4,128)S(1)}, s32[256,4]{0,1:T(4,128)}, u32[]{:S(2)}) copy-start(s32[256,4]{0,1:T(4,128)} %param.30) | copy-start | bytes 12292
  103.7 6.2 %collective-permute-start.23 = (bf16[32,2048]{1,0:T(8,128)(2,1)S(1)}, bf16[32,2048]{1,0:T(8,128)(2,1)S(1)}, u32[]{:S(2)}, u32[]{:S(2)}) collective-permute-start(bf16[32,2048]{1,0:T(8,128)(2,1)S(1)} %get-tuple-element.71.refs_0_), channel_id=1, source_target_pairs={{0,2},{2,4},{4,6},{6,0},{1,3},{3,5},{5,7},{7,1},{8,10},{10,12},{12... | collective-permute-start | bytes 393224 | tf_op jit(solution)/shard_map/ppermute | solution.py:29
  104.1 7.6 %collective-permute-start.24 = (bf16[32,2048]{1,0:T(8,128)(2,1)S(1)}, bf16[32,2048]{1,0:T(8,128)(2,1)S(1)}, u32[]{:S(2)}, u32[]{:S(2)}) collective-permute-start(bf16[32,2048]{1,0:T(8,128)(2,1)S(1)} %get-tuple-element.71.refs_0_), channel_id=1, source_target_pairs={{0,6},{2,0},{4,2},{6,4},{1,7},{3,1},{5,3},{7,5},{8,14},{10,8},{12,... | collective-permute-start | bytes 393224 | tf_op jit(solution)/shard_map/ppermute | solution.py:29
  106.9 6.5 %collective-permute-start.25 = (bf16[32,2048]{1,0:T(8,128)(2,1)S(1)}, bf16[32,2048]{1,0:T(8,128)(2,1)S(1)}, u32[]{:S(2)}, u32[]{:S(2)}) collective-permute-start(bf16[32,2048]{1,0:T(8,128)(2,1)S(1)} %get-tuple-element.71.refs_0_), channel_id=1, source_target_pairs={{0,4},{2,6},{4,0},{6,2},{1,5},{3,7},{5,1},{7,3},{8,12},{10,14},{12... | collective-permute-start | bytes 393224 | tf_op jit(solution)/shard_map/ppermute | solution.py:29
  107.2 8.3 %collective-permute-start.26 = (bf16[32,2048]{1,0:T(8,128)(2,1)S(1)}, bf16[32,2048]{1,0:T(8,128)(2,1)S(1)}, u32[]{:S(2)}, u32[]{:S(2)}) collective-permute-start(bf16[32,2048]{1,0:T(8,128)(2,1)S(1)} %get-tuple-element.71.refs_0_), channel_id=1, source_target_pairs={{0,1},{1,0},{2,3},{3,2},{4,5},{5,4},{6,7},{7,6},{8,9},{9,8},{10,11... | collective-permute-start | bytes 393224 | tf_op jit(solution)/shard_map/ppermute | solution.py:29
  109.8 5.7 %collective-permute-start.27 = (bf16[32,2048]{1,0:T(8,128)(2,1)S(1)}, bf16[32,2048]{1,0:T(8,128)(2,1)S(1)}, u32[]{:S(2)}, u32[]{:S(2)}) collective-permute-start(bf16[32,2048]{1,0:T(8,128)(2,1)S(1)} %collective-permute-done.23.refs_1_), channel_id=1, source_target_pairs={{0,1},{1,0},{2,3},{3,2},{4,5},{5,4},{6,7},{7,6},{8,9},{9,8},{10,11... | collective-permute-start | bytes 393224 | tf_op jit(solution)/shard_map/ppermute | solution.py:29
  111.8 3.8 %collective-permute-start.28 = (bf16[32,2048]{1,0:T(8,128)(2,1)S(1)}, bf16[32,2048]{1,0:T(8,128)(2,1)S(1)}, u32[]{:S(2)}, u32[]{:S(2)}) collective-permute-start(bf16[32,2048]{1,0:T(8,128)(2,1)S(1)} %collective-permute-done.24.refs_2_), channel_id=1, source_target_pairs={{0,1},{1,0},{2,3},{3,2},{4,5},{5,4},{6,7},{7,6},{8,9},{9,8},{10,11... | collective-permute-start | bytes 393224 | tf_op jit(solution)/shard_map/ppermute | solution.py:29
  113.4 2.2 %collective-permute-start.29 = (bf16[32,2048]{1,0:T(8,128)(2,1)S(1)}, bf16[32,2048]{1,0:T(8,128)(2,1)S(1)}, u32[]{:S(2)}, u32[]{:S(2)}) collective-permute-start(bf16[32,2048]{1,0:T(8,128)(2,1)S(1)} %collective-permute-done.25.refs_3_), channel_id=1, source_target_pairs={{0,1},{1,0},{2,3},{3,2},{4,5},{5,4},{6,7},{7,6},{8,9},{9,8},{10,11... | collective-permute-start | bytes 393224 | tf_op jit(solution)/shard_map/ppermute | solution.py:29
  154.0 1.6 copy-start.2
  155.6 1.6 copy-start.3
  157.2 1.6 copy-start.4
  162.6 6.4 %copy-start.16 = (bf16[2048,64]{0,1:T(8,128)(2,1)S(1)}, bf16[2048,64]{0,1:T(8,128)(2,1)}, u32[]{:S(2)}) copy-start(bf16[2048,64]{0,1:T(8,128)(2,1)} %param.35) | copy-start | bytes 786436
  162.6 6.7 %copy-start.17 = (bf16[2048,64]{0,1:T(8,128)(2,1)S(1)}, bf16[2048,64]{0,1:T(8,128)(2,1)}, u32[]{:S(2)}) copy-start(bf16[2048,64]{0,1:T(8,128)(2,1)} %param.36) | copy-start | bytes 786436
  162.6 7.7 %copy-start.10 = (bf16[64,2048]{1,0:T(8,128)(2,1)S(1)}, bf16[64,2048]{1,0:T(8,128)(2,1)}, u32[]{:S(2)}) copy-start(bf16[64,2048]{1,0:T(8,128)(2,1)} %down.3) | copy-start | bytes 786436
  162.6 33.8 %all-to-all-start.2 = ((bf16[32,8,2048]{2,1,0:T(8,128)(2,1)}), bf16[32,8,2048]{2,1,0:T(8,128)(2,1)}, u32[]{:S(2)}, u32[]{:S(2)}) async-start(bf16[32,8,2048]{2,1,0:T(8,128)(2,1)} %bitcast.11), calls=%async_computation.2 | async-start | bytes 2097152 | tf_op jit(solution)/shard_map/all_to_all | solution.py:541
  174.5 36.3 %copy-start.9 = (f32[32,2048]{1,0:T(8,128)S(1)}, f32[32,2048]{1,0:T(8,128)}, u32[]{:S(2)}) copy-start(f32[32,2048]{1,0:T(8,128)} %copy-done.8) | copy-start | bytes 786436
  198.3 2.0 collective-permute-start.30
  201.0 6.8 %collective-permute-start.31 = (bf16[32,2048]{1,0:T(8,128)(2,1)S(1)}, bf16[32,2048]{1,0:T(8,128)(2,1)S(1)}, u32[]{:S(2)}, u32[]{:S(2)}) collective-permute-start(bf16[32,2048]{1,0:T(8,128)(2,1)S(1)} %get-tuple-element.78), channel_id=1, source_target_pairs={{0,2},{2,4},{4,6},{6,0},{1,3},{3,5},{5,7},{7,1},{8,10},{10,12},{12... | collective-permute-start | bytes 393224 | tf_op jit(solution)/shard_map/ppermute | solution.py:29
  201.1 8.8 %collective-permute-start.32 = (bf16[32,2048]{1,0:T(8,128)(2,1)S(1)}, bf16[32,2048]{1,0:T(8,128)(2,1)S(1)}, u32[]{:S(2)}, u32[]{:S(2)}) collective-permute-start(bf16[32,2048]{1,0:T(8,128)(2,1)S(1)} %get-tuple-element.79), channel_id=1, source_target_pairs={{0,6},{2,0},{4,2},{6,4},{1,7},{3,1},{5,3},{7,5},{8,14},{10,8},{12,... | collective-permute-start | bytes 393224 | tf_op jit(solution)/shard_map/ppermute | solution.py:29
  204.3 6.5 %collective-permute-start.33 = (bf16[32,2048]{1,0:T(8,128)(2,1)S(1)}, bf16[32,2048]{1,0:T(8,128)(2,1)S(1)}, u32[]{:S(2)}, u32[]{:S(2)}) collective-permute-start(bf16[32,2048]{1,0:T(8,128)(2,1)S(1)} %get-tuple-element.80), channel_id=1, source_target_pairs={{0,4},{2,6},{4,0},{6,2},{1,5},{3,7},{5,1},{7,3},{8,12},{10,14},{12... | collective-permute-start | bytes 393224 | tf_op jit(solution)/shard_map/ppermute | solution.py:29
  (7 other events, 6.5 us)
